TPU v7x, 512 devices: a whole 4x4x16 slice. The times are simulated.
512 devices in a mesh: sp: 16 (over z), fs: 4 (over y), tp: 8 (over x, core).
Axes of the slice: x: 4, y: 4, z: 16, core: 2. Of those that a mesh axis runs over, the one named last changes fastest.
Arguments:
- tokens: bfloat16 [4, 16384, 2048], P('fs', 'sp', 'tp'), may hold values from -8 to 8
- norm_gain: float32 [2048], replicated, may hold values from 0.1 to 1.9
- w_query: bfloat16 [2048, 1024], P(('sp', 'fs'), 'tp'), may hold values from -4 to 4
- w_key: bfloat16 [2048, 512], P(('sp', 'fs'), 'tp'), may hold values from -0.16 to 0.16
- w_value: bfloat16 [2048, 512], P(('sp', 'fs'), 'tp'), may hold values from -0.125 to 0.125
- w_conv_in: bfloat16 [2048, 1024], P(('sp', 'fs'), 'tp'), may hold values from -0.125 to 0.125
- w_conv_b: bfloat16 [2048, 1024], P(('sp', 'fs'), 'tp'), may hold values from -0.125 to 0.125
- w_conv_c: bfloat16 [2048, 1024], P(('sp', 'fs'), 'tp'), may hold values from -0.125 to 0.125
- conv_taps: bfloat16 [3, 1024], P(None, 'tp'), may hold values from -3.5 to 3.5
- sink_logits: float32 [16], P('tp'), may hold values from 1 to 5
- w_attn_out: bfloat16 [1024, 2048], P('tp', ('sp', 'fs')), may hold values from -0.375 to 0.375
- w_conv_out: bfloat16 [1024, 2048], P('tp', ('sp', 'fs')), may hold values from -0.125 to 0.125
Outputs:
- mixed: bfloat16 [4, 16384, 2048], P('fs', ('sp', 'tp'))
All inputs are finite; a program needn't handle non-finite values.
Results may differ from a plain program's by a relative error of at most 0.02.
Values may be sent and summed in bfloat16 or wider, within the bound.
A program may use at most 128 MiB of HBM per device.

v0:
```python
import jax
import jax.numpy as jnp
from jax import lax
from jax.sharding import PartitionSpec as P

HEADS = 16
HEAD = 64
WINDOW = 128


def in_one_piece(arrays, axis, dim, along):
    widths = [a.shape[along] for a in arrays]
    both = jnp.concatenate(arrays, axis=along)
    whole = lax.all_gather(both, axis, axis=dim, tiled=True)
    return tuple(jnp.split(whole, [sum(widths[:k]) for k in range(1, len(widths))], axis=along))


def shifted(block, axis, distance):
    devices = range(lax.axis_size(axis))
    route = [(i - distance, i) for i in devices if i - distance in devices]
    return lax.ppermute(block, axis, route)


def rows_first(arrays, axis, dims):
    turned = [jnp.moveaxis(a, dim, 0) for a, dim in zip(arrays, dims)]
    both = jnp.concatenate([t.reshape(len(t), -1) for t in turned], axis=1)
    whole, at, finished = (lax.all_gather(both, axis, axis=0, tiled=True), 0, [])
    for t, dim in zip(turned, dims):
        share = whole[:, at : at + t[0].size].reshape(-1, *t.shape[1:])
        finished.append(jnp.moveaxis(share, 0, dim))
        at += t[0].size
    return tuple(finished)


def norm_rows(tokens, norm_gain):
    values = tokens.astype(jnp.float32)
    average = jnp.mean(values, axis=-1, keepdims=True)
    centred = values - average
    variance = jnp.mean(centred * centred, axis=-1, keepdims=True)
    return (centred * lax.rsqrt(variance + 1e-05) * norm_gain).astype(jnp.bfloat16)


def attend(queries, keys_values, earlier_rows, sink_logits, head_base, row_base):
    row_total = queries.shape[0]
    kv_cols = keys_values.shape[1] // 2
    kv_here = kv_cols // HEAD
    heads_here = queries.shape[1] // HEAD
    group = heads_here // kv_here
    keys_all = jnp.concatenate([earlier_rows, keys_values], axis=0)
    block_rows = min(512, row_total)
    head_ids = head_base + jnp.arange(heads_here, dtype=jnp.int32)
    slopes = jnp.exp2(-8.0 * (head_ids + 1).astype(jnp.float32) / HEADS).reshape(kv_here, group)[
        :, :, None, None
    ]
    sinks = sink_logits.reshape(kv_here, group)[:, :, None, None]
    row_ids = jnp.arange(block_rows, dtype=jnp.int32)[:, None]
    col_ids = jnp.arange(block_rows + WINDOW, dtype=jnp.int32)[None, :]
    distance = WINDOW + row_ids - col_ids
    outputs = []
    for block in range(row_total // block_rows):
        first_row = block * block_rows
        query_block = queries[first_row : first_row + block_rows].reshape(
            block_rows, kv_here, group, HEAD
        )
        band = keys_all[first_row : first_row + block_rows + WINDOW]
        band_keys = band[:, :kv_cols].reshape(block_rows + WINDOW, kv_here, HEAD)
        band_values = band[:, kv_cols:].reshape(block_rows + WINDOW, kv_here, HEAD)
        scores = jnp.einsum(
            "qkgd,skd->kgqs", query_block, band_keys, preferred_element_type=jnp.float32
        ) * HEAD ** (-0.5)
        scores = scores - slopes * distance.astype(jnp.float32)
        key_place = row_base + first_row - WINDOW + col_ids
        keep = (distance >= 0) & (distance < WINDOW) & (key_place >= 0)
        scores = jnp.where(keep, scores, -jnp.inf)
        highest = jnp.maximum(jnp.max(scores, axis=-1, keepdims=True), sinks)
        raised = jnp.exp(scores - highest)
        denominator = jnp.sum(raised, axis=-1, keepdims=True) + jnp.exp(sinks - highest)
        weights = (raised / denominator).astype(jnp.bfloat16)
        mixed = jnp.einsum(
            "kgqs,skd->qkgd", weights, band_values, preferred_element_type=jnp.float32
        )
        outputs.append(mixed.astype(jnp.bfloat16).reshape(block_rows, heads_here * HEAD))
    return jnp.concatenate(outputs, axis=0)


def on_device(
    tokens,
    norm_gain,
    w_query,
    w_key,
    w_value,
    w_conv_in,
    w_conv_b,
    w_conv_c,
    conv_taps,
    sink_logits,
    w_attn_out,
    w_conv_out,
):
    gathered = lax.all_gather(tokens, "tp", axis=2, tiled=True)[0]
    normed = norm_rows(gathered, norm_gain)
    row_total = normed.shape[0]
    weight_rows = in_one_piece(
        (w_query, w_key, w_value, w_conv_in, w_conv_b, w_conv_c), ("sp", "fs"), 0, 1
    )
    results = tuple(
        (
            jnp.dot(normed, rows_part, preferred_element_type=jnp.float32)
            for rows_part in weight_rows
        )
    )
    queries, keys, values, inner, gate_b, gate_c = tuple(
        (result.astype(jnp.bfloat16) for result in results)
    )
    product = (gate_c.astype(jnp.float32) * inner.astype(jnp.float32)).astype(jnp.bfloat16)
    keys_values = jnp.concatenate([keys, values], axis=1)
    earlier_kv, earlier_product = shifted(
        (keys_values[row_total - WINDOW :], product[row_total - 2 :]), "sp", 1
    )
    heads_here = queries.shape[1] // HEAD
    head_base = lax.axis_index("tp") * heads_here
    row_base = lax.axis_index("sp") * row_total
    attended = attend(queries, keys_values, earlier_kv, sink_logits, head_base, row_base)
    taps = conv_taps.astype(jnp.float32)
    padded = jnp.concatenate([earlier_product, product], axis=0).astype(jnp.float32)
    filtered = (
        taps[0] * padded[0:row_total]
        + taps[1] * padded[1 : row_total + 1]
        + taps[2] * padded[2 : row_total + 2]
    )
    conv_out = (gate_b.astype(jnp.float32) * filtered).astype(jnp.bfloat16)
    attn_columns, conv_columns = rows_first((w_attn_out, w_conv_out), ("sp", "fs"), (1, 1))
    summed = lax.psum_scatter(
        (
            jnp.dot(attended, attn_columns, preferred_element_type=jnp.float32)
            + jnp.dot(conv_out, conv_columns, preferred_element_type=jnp.float32)
        ).astype(jnp.bfloat16),
        "tp",
        scatter_dimension=0,
        tiled=True,
    )
    return summed[None]


def solution(mesh):
    placed = (
        P("fs", "sp", "tp"),
        P(),
        P(("sp", "fs"), "tp"),
        P(("sp", "fs"), "tp"),
        P(("sp", "fs"), "tp"),
        P(("sp", "fs"), "tp"),
        P(("sp", "fs"), "tp"),
        P(("sp", "fs"), "tp"),
        P(None, "tp"),
        P("tp"),
        P("tp", ("sp", "fs")),
        P("tp", ("sp", "fs")),
    )
    return jax.shard_map(
        on_device,
        mesh=mesh,
        in_specs=placed,
        out_specs=P("fs", ("sp", "tp"), None),
        check_vma=False,
    )
```

profile of v0, /device:TPU:1, one launch (start us, length us, event | category | flops | bytes accessed | tf_op | source)
XLA Modules:
  0.0 405.3 jit_solution(2349871307167087293)
XLA Ops:
  6.5 0.0 all-gather.4.cloned.1.call-start
  6.5 0.7 all-gather.4.cloned.1.call-update
  7.3 0.0 all-gather.6.cloned.1.call-start
  7.3 1.5 concatenate.18
  8.8 0.0 all-gather.6.cloned.1.call-update
  8.8 0.0 all-gather.8.cloned.1.call-start
  8.9 1.3 pad_maximum_fusion.4
  10.2 0.0 all-gather.8.cloned.1.call-update
  10.2 0.0 reduce-scatter.2.cloned.1.call-start
  10.3 0.7 convert_element_type.108
  11.0 1.2 fusion.14
  12.2 0.5 fusion.32
  12.7 45.6 %all-gather.4.cloned.1.call-done = bf16[1,1024,2048]{2,1,0:T(8,128)(2,1)} async-done(((bf16[1,1024,256]{2,1,0:T(8,128)(2,1)}), bf16[1,1024,2048]{2,1,0:T(8,128)(2,1)}) %all-gather.4.cloned.1.call-update) | async-done | bytes 4194320 | tf_op jit(solution)/shard_map/all_gather | solution.py:100
  58.3 3.0 convert_reduce_fusion
  61.3 0.0 copy-start.4
  61.3 0.5 copy-done.1
  61.8 1.2 fusion.3
  63.0 0.0 copy-done.4
  63.0 3.0 fusion.5
  66.0 128.8 %all-gather.6.cloned.1.call-done = bf16[2048,640]{1,0:T(8,128)(2,1)} async-done(((bf16[32,640]{1,0:T(8,128)(2,1)}), bf16[2048,640]{1,0:T(8,128)(2,1)}) %all-gather.6.cloned.1.call-update) | async-done | bytes 2621456 | tf_op jit(solution)/shard_map/all_gather | solution.py:14
  194.8 3.9 convolution_convert_fusion.4
  198.8 0.0 copy-done
  198.8 0.0 copy-start.2
  198.8 2.6 convolution_convert_fusion.5
  201.4 2.9 collective-permute-start
  204.3 0.0 copy-done.2
  204.3 1.5 convolution_convert_fusion.3
  205.8 1.2 fusion.21
  207.1 1.3 fusion.20
  208.4 2.7 collective-permute-start.1
  211.1 0.9 fusion.65
  212.0 0.0 copy-start.5
  212.0 0.0 collective-permute-done.1
  212.0 0.1 maximum_convert_fusion
  212.1 0.0 collective-permute-done
  212.1 0.9 fusion.64
  213.0 0.1 broadcast_maximum_fusion.1
  213.1 0.4 fusion.8
  213.4 0.1 exponential_add_fusion.1
  213.5 0.4 fusion.9
  213.9 0.1 exponential_add_fusion
  214.0 0.6 fusion.28
  214.5 0.6 fusion.25
  215.1 117.1 %all-gather.8.cloned.1.call-done = bf16[2048,256]{1,0:T(8,128)(2,1)} async-done(((bf16[32,256]{1,0:T(8,128)(2,1)}), bf16[2048,256]{1,0:T(8,128)(2,1)}) %all-gather.8.cloned.1.call-update) | async-done | bytes 1048592 | tf_op jit(solution)/shard_map/all_gather | solution.py:27
  332.2 5.6 %fusion.42 = f32[1024,2048]{1,0:T(8,128)} fusion(bf16[2048,256]{1,0:T(8,128)(2,1)} %all-gather.8.cloned.1.call-done, bf16[512,128]{0,1:T(8,128)(2,1)S(1)} %bitcast.77, bf16[512,128]{0,1:T(8,128)(2,1)S(1)} %bitcast.78), kind=kOutput, calls=%fused_computation.54 | convolution fusion | flops 537395200 | bytes 9175040 | tf_op jit(solution)/shard_map/dot_general | solution.py:135
  337.7 11.1 %add_convert_fusion = bf16[1024,2048]{1,0:T(8,128)(2,1)} fusion(f32[1024,2048]{1,0:T(8,128)} %fusion.42, bf16[1024,2048]{1,0:T(8,128)(2,1)} %fusion.5, bf16[2048,256]{1,0:T(8,128)(2,1)} %all-gather.8.cloned.1.call-done, f32[1026,128]{1,0:T(8,128)S(1)} %maximum_convert_fusion, bf16[2048,640]{1,0:T(8,128)(2,1)S(1)} %copy-done.2, f32[128]{0:T(128)S(1)} %get-tuple-element.8, ...), kind=kOutput, calls=%fused_computation.8 | convolution fusion | flops 1079115776 | bytes 19400192 | tf_op jit(solution)/shard_map/dot_general | solution.py:136
  348.9 0.0 reduce-scatter.2.cloned.1.call-update
  348.9 49.9 %reduce-scatter.2.cloned.1.call-done = bf16[128,2048]{1,0:T(8,128)(2,1)} async-done(((bf16[1024,2048]{1,0:T(8,128)(2,1)}), bf16[128,2048]{1,0:T(8,128)(2,1)}) %reduce-scatter.2.cloned.1.call-update) | async-done | bytes 524304 | tf_op jit(solution)/shard_map/reduce_scatter | solution.py:133
  (14 shorter events, 0.1 us)
Async XLA Ops:
  6.5 51.8 %all-gather.4.cloned.1.call-start = ((), (), s32[]{:S(2)}) async-start(), calls=%async_computation.1 | async-start | bytes 4718592 | tf_op jit(solution)/shard_map/all_gather | solution.py:100
  7.3 187.6 %all-gather.6.cloned.1.call-start = ((), (), s32[]{:S(2)}) async-start(), calls=%async_computation.2 | async-start | bytes 2662400 | tf_op jit(solution)/shard_map/all_gather | solution.py:14
  8.8 323.4 %all-gather.8.cloned.1.call-start = ((), (), s32[]{:S(2)}) async-start(), calls=%async_computation.3 | async-start | bytes 1064960 | tf_op jit(solution)/shard_map/all_gather | solution.py:27
  10.2 388.6 %reduce-scatter.2.cloned.1.call-start = ((), (), s32[]{:S(2)}) async-start(), calls=%async_computation.4 | async-start | bytes 4718592 | tf_op jit(solution)/shard_map/reduce_scatter | solution.py:133
  58.3 3.4 copy-start.1
  61.3 1.7 copy-start.4
  194.8 3.9 copy-start
  198.8 5.5 %copy-start.2 = (bf16[2048,640]{1,0:T(8,128)(2,1)S(1)}, bf16[2048,640]{1,0:T(8,128)(2,1)}, u32[]{:S(2)}) copy-start(bf16[2048,640]{1,0:T(8,128)(2,1)} %all-gather.6.cloned.1.call-done) | copy-start | bytes 7864324
  201.4 10.7 %collective-permute-start = (bf16[128,128]{0,1:T(8,128)(2,1)S(1)}, bf16[128,128]{0,1:T(8,128)(2,1)S(1)}, u32[]{:S(2)}, u32[]{:S(2)}) collective-permute-start(bf16[128,128]{0,1:T(8,128)(2,1)S(1)} %pad_maximum_fusion.3), channel_id=1, source_target_pairs={{0,32},{32,64},{64,96},{96,128},{128,160},{160,192},{192,224},{224... | collective-permute-start | bytes 98312 | tf_op jit(solution)/shard_map/ppermute | solution.py:21
  207.1 4.0 copy-start.3
  208.4 3.6 collective-permute-start.1
  212.0 1.0 copy-start.5
Sparse Core Ops, SparseCore 0:
  9.4 48.8 all-gather.3
  61.3 133.5 all-gather.5
  197.8 134.3 all-gather.7
  349.0 49.7 reduce-scatter.1
where the time goes:
time: 407 us; the launch traced here: 405 us
  waiting for transfers between devices  342 us (84%)
  matrix products  30.1 us (7%)
  between operations  13.4 us (3%)
  other arithmetic  12 us (3%)
  starting transfers between devices  5.74 us (1%)
    all_gather x1, waiting for transfers between devices, in_one_piece(): whole = lax.all_gather(both, axis, axis=dim, tiled=True)  129 us
    all_gather x1, waiting for transfers between devices, rows_first(): lax.all_gather(both, axis, axis=0, tiled=True)  117 us
    reduce_scatter x1, waiting for transfers between devices, on_device(): lax.psum_scatter((jnp.dot(attended, attn_columns, preferred_element_type=...  49.9 us
    all_gather x1, waiting for transfers between devices, on_device(): gathered = lax.all_gather(tokens, 'tp', axis=2, tiled=True)[0]  45.6 us
    dot_general x1, matrix products, on_device(): jnp.dot(conv_out, conv_columns, preferred_element_type=jnp.float32)  11.1 us
    dot_general x5, matrix products, on_device(): jnp.dot(normed, rows_part, preferred_element_type=jnp.float32)  10.5 us
  transfers between devices with their start and end apart: 6, of which 4 were waited for; matrix products, arithmetic and copies ran while one was open for 7% of the time, Pallas kernels for 0%

commit v1 on v0

v1 whole, which is shorter than its diff:
```python
import functools

import jax
import jax.numpy as jnp
from jax import lax
from jax.experimental import pallas as pl
from jax.experimental.pallas import tpu as pltpu
from jax.sharding import PartitionSpec as P

HEADS = 16
HEAD = 64
WINDOW = 128
NZ, NY, NX = 16, 4, 4
MESH = pl.DeviceIdType.MESH
NT = (((1,), (1,)), ((), ()))

STREAMS = (("zy", 256), ("zy", 384), ("zy", 384), ("yz", 256), ("yz", 384))
UP = (8, 7, 8, 7, 8)


def kernel(
    tok, gain, wq, wk, wv, wi, wb, wc, taps, sinks, wao, wco,
    out,
    T, N, B0, B1, B2, B3, B4, Q, KV, PR, GB, BIAS, AALL, AOUT, XS, XR, ACC, OUTV,
    lsem, osem, zs, zr, ys, yr, ays, ayr, xs, xr, ds, dr, oxs, oxr, hs, hr, as_, ar, es, er,
):
    z = lax.axis_index("sp")
    y = lax.axis_index("fs")
    t = lax.axis_index("tp")
    x = t // 2
    c = t % 2
    bufs = (B0, B1, B2, B3, B4)

    def dev(dz=0, dy=0, dx=0):
        return (
            lax.rem(z + NZ + dz, NZ),
            lax.rem(y + NY + dy, NY),
            lax.rem(x + NX + dx, NX) * 2 + c,
        )

    partner = (z, y, x * 2 + (1 - c))

    def rc(src, dst, ssem, rsem, to):
        return pltpu.make_async_remote_copy(
            src_ref=src, dst_ref=dst, send_sem=ssem, recv_sem=rsem, device_id=to, device_id_type=MESH
        )

    def tload(i):
        rows = pl.ds(256 * i, 256)
        return pltpu.make_async_copy(tok.at[rows, :], T.at[t, rows, :], lsem.at[i])

    for i in range(4):
        tload(i).start()

    own = pl.ds(pl.multiple_of(32 * (NY * z + y), 32), 32)
    B0[own, 0:128] = wq[...]
    B0[own, 128:256] = jnp.concatenate([wk[...], wv[...]], axis=1)
    B1[own, 0:128] = wi[...]
    B1[own, 128:256] = wb[...]
    B1[own, 256:384] = wc[...]
    B3[own, 0:128] = wao[...]
    B3[own, 128:256] = wco[...]

    barrier = pltpu.get_barrier_semaphore()
    peers = [dev(dz=1), dev(dz=-1), dev(dy=1), dev(dy=-1), dev(dx=1), dev(dx=-1), dev(dx=2), partner]
    for peer in peers:
        pl.semaphore_signal(barrier, inc=1, device_id=peer, device_id_type=MESH)
    pl.semaphore_wait(barrier, len(peers))

    def zblock(st, b):
        buf = bufs[st]
        if STREAMS[st][0] == "zy":
            return buf.at[pl.ds(pl.multiple_of(32 * (NY * b + y), 32), 32), :]
        return buf.at[pl.ds(pl.multiple_of(128 * b, 128), 128), :]

    def yblock(st, b, dy):
        yy = lax.rem(y + NY + dy, NY)
        return bufs[st].at[pl.ds(pl.multiple_of(32 * (NY * b + yy), 32), 32), :]

    def steps(st, way):
        return UP[st] if way == 0 else 15 - UP[st]

    def origin(way, s):
        return lax.rem(z + NZ - s, NZ) if way == 0 else lax.rem(z + s, NZ)

    def zcopy(st, way, s, recv):
        ref = zblock(st, origin(way, s + 1 if recv else s))
        return rc(ref, ref, zs.at[st, way, s], zr.at[st, way, s], dev(dz=1 if way == 0 else -1))

    def z_send(st, s):
        for way in (0, 1):
            if s < steps(st, way):
                zcopy(st, way, s, False).start()

    def z_wait(st, s):
        for way in (0, 1):
            if s < steps(st, way):
                zcopy(st, way, s, True).wait_recv()

    def slots(st, s):
        if s < 0:
            return [(0, 0, 0)]
        return [(1 + 8 * way + s, way, s + 1) for way in (0, 1) if s < steps(st, way)]

    def ycopy(st, slot, b, k, recv):
        if k == 2:
            fwd_up = slot < 9
            if recv:
                ref = yblock(st, b, 2)
            else:
                ref = yblock(st, b, -1 if fwd_up else 1)
            to = dev(dy=1 if fwd_up else -1)
        else:
            ref = yblock(st, b, 0 if not recv else (-1 if k == 0 else 1))
            to = dev(dy=1 if k == 0 else -1)
        return rc(ref, ref, ys.at[st, slot, k], yr.at[st, slot, k], to)

    def y_send(st, s):
        for slot, way, d in slots(st, s):
            for k in (0, 1):
                ycopy(st, slot, origin(way, d), k, False).start()

    def y_fwd(st, s):
        for slot, way, d in slots(st, s):
            b = origin(way, d)
            first = 0 if slot < 9 else 1
            ycopy(st, slot, b, first, True).wait_recv()
            ycopy(st, slot, b, 2, False).start()

    def y_fin(st, s):
        for slot, way, d in slots(st, s):
            b = origin(way, d)
            ycopy(st, slot, b, 1 if slot < 9 else 0, True).wait_recv()
            ycopy(st, slot, b, 2, True).wait_recv()

    def aycopy(st, k, recv):
        up = st % 2 == 0
        if k == 2:
            ref = yblock(st, z, 2) if recv else yblock(st, z, -1 if up else 1)
            to = dev(dy=1 if up else -1)
        else:
            ref = yblock(st, z, 0 if not recv else (-1 if k == 0 else 1))
            to = dev(dy=1 if k == 0 else -1)
        return rc(ref, ref, ays.at[st - 3, k], ayr.at[st - 3, k], to)

    def ay_send(st):
        aycopy(st, 0, False).start()
        aycopy(st, 1, False).start()

    def ay_fwd(st):
        first = 0 if st % 2 == 0 else 1
        aycopy(st, first, True).wait_recv()
        aycopy(st, 2, False).start()
        aycopy(st, 1 - first, True).wait_recv()

    def ay_fin(st):
        aycopy(st, 2, True).wait_recv()

    ox_parts = (
        (1, 0, 256, 4, 0), (2, 0, 128, 4, 256), (2, 128, 256, 2, 0), (3, 0, 256, 2, 128),
    )

    def oxcopy(k):
        d, lo, hi, st, at = ox_parts[k]
        return rc(
            B3.at[own, lo:hi], bufs[st].at[own, at : at + hi - lo], oxs.at[k], oxr.at[k], dev(dx=-d)
        )

    def tchunk(i, dx, cc):
        tt = lax.rem(x + NX + dx, NX) * 2 + cc
        return T.at[tt, pl.ds(256 * i, 256), :]

    def tcopy(i, k, recv):
        up = i % 2 == 0
        if k == 2:
            ref = tchunk(i, 2, c) if recv else tchunk(i, -1 if up else 1, c)
            to = dev(dx=1 if up else -1)
        else:
            ref = tchunk(i, 0 if not recv else (-1 if k == 0 else 1), c)
            to = dev(dx=1 if k == 0 else -1)
        return rc(ref, ref, xs.at[i, k], xr.at[i, k], to)

    def dcopy(i, k, recv):
        ref = tchunk(i, (0, -1, 1, 2)[k], c if not recv else 1 - c)
        return rc(ref, ref, ds.at[i, k], dr.at[i, k], partner)

    def t_send(i):
        tload(i).wait()
        tcopy(i, 0, False).start()
        tcopy(i, 1, False).start()
        dcopy(i, 0, False).start()

    def t_fwd(i):
        up = i % 2 == 0
        first = 0 if up else 1
        tcopy(i, first, True).wait_recv()
        tcopy(i, 2, False).start()
        dcopy(i, 1 + first, False).start()
        tcopy(i, 1 - first, True).wait_recv()
        dcopy(i, 2 - first, False).start()

    def t_fwd2(i):
        tcopy(i, 2, True).wait_recv()
        dcopy(i, 3, False).start()

    def t_fin(i):
        for k in range(4):
            dcopy(i, k, True).wait_recv()

    def norm(i):
        @pl.loop(0, 8)
        def _(j):
            rows = pl.ds(pl.multiple_of(256 * i + 32 * j, 32), 32)
            total = T[0, rows, :].astype(jnp.float32)
            for k in range(1, 8):
                total += T[k, rows, :].astype(jnp.float32)
            average = jnp.sum(total, axis=1, keepdims=True) * (1.0 / 2048)
            squares = jnp.zeros((32, 256), jnp.float32)
            for k in range(8):
                centred = T[k, rows, :].astype(jnp.float32) - average
                squares += centred * centred
            variance = jnp.sum(squares, axis=1, keepdims=True) * (1.0 / 2048)
            scale = lax.rsqrt(variance + 1e-05)
            for k in range(8):
                centred = T[k, rows, :].astype(jnp.float32) - average
                cols = slice(256 * k, 256 * k + 256)
                N[rows, cols] = (centred * scale * gain[:, cols]).astype(jnp.bfloat16)

    def project(i):
        rows = slice(256 * i, 256 * i + 256)
        normed = N[rows, :]
        qkv = jnp.dot(normed, B0[...], preferred_element_type=jnp.float32)
        Q[rows, :] = qkv[:, 0:128].astype(jnp.bfloat16)
        KV[128 + 256 * i : 128 + 256 * i + 256, :] = qkv[:, 128:256].astype(jnp.bfloat16)
        ibc = jnp.dot(normed, B1[...], preferred_element_type=jnp.float32).astype(jnp.bfloat16)
        inner = ibc[:, 0:128].astype(jnp.float32)
        gate_c = ibc[:, 256:384].astype(jnp.float32)
        product = (gate_c * inner).astype(jnp.bfloat16)
        PR[16 + 256 * i : 16 + 256 * i + 256, :] = product.astype(jnp.float32)
        GB[rows, :] = ibc[:, 128:256]

    def halo(k):
        to = dev(dz=1)
        if k == 0:
            return rc(KV.at[1024:1152, :], KV.at[0:128, :], hs.at[0], hr.at[0], to)
        return rc(PR.at[1032:1040, :], PR.at[8:16, :], hs.at[1], hr.at[1], to)

    def bias_init():
        row = lax.broadcasted_iota(jnp.int32, (128, 512), 0)
        col = lax.broadcasted_iota(jnp.int32, (128, 512), 1)
        upper = col >= 256
        distance = 128 + row - jnp.where(upper, col - 256, col)
        head = jnp.where(upper, 1, 0) + 2 * t
        slope = jnp.exp2((head + 1).astype(jnp.float32) * (-8.0 / HEADS))
        keep = (distance >= 0) & (distance < WINDOW)
        BIAS[...] = jnp.where(keep, -slope * distance.astype(jnp.float32), -jnp.inf)

    def mix(k):
        r0 = pl.multiple_of(256 * lax.rem(x + k, NX), 256)
        lane = lax.broadcasted_iota(jnp.int32, (256, 128), 1)
        low = lane < 64
        for sub in range(2):
            q0 = pl.multiple_of(r0 + 128 * sub, 128)
            q = Q[pl.ds(q0, 128), :]
            kv = KV[pl.ds(q0, 256), :].astype(jnp.float32)
            vk = pltpu.roll(kv, 64, 1)
            keys = jnp.concatenate(
                [jnp.where(low, kv, 0.0), jnp.where(low, 0.0, vk)], axis=0
            ).astype(jnp.bfloat16)
            values = jnp.concatenate(
                [jnp.where(low, vk, 0.0), jnp.where(low, 0.0, kv)], axis=0
            ).astype(jnp.bfloat16)
            scores = lax.dot_general(q, keys, NT, preferred_element_type=jnp.float32)
            scores = scores * HEAD ** (-0.5) + BIAS[...]
            if sub == 0:
                col = lax.broadcasted_iota(jnp.int32, (128, 512), 1)
                place = jnp.bitwise_and(col, 255) + (1024 * z + r0 - WINDOW)
                scores = jnp.where(place >= 0, scores, -jnp.inf)
            weights = []
            for g in range(2):
                part = scores[:, 256 * g : 256 * g + 256]
                sink = sinks[0, g]
                top = jnp.maximum(jnp.max(part, axis=1, keepdims=True), sink)
                raised = jnp.exp(part - top)
                below = jnp.sum(raised, axis=1, keepdims=True) + jnp.exp(sink - top)
                weights.append((raised * (1.0 / below)).astype(jnp.bfloat16))
            attended = jnp.dot(
                jnp.concatenate(weights, axis=1), values, preferred_element_type=jnp.float32
            )
            AOUT[k, 128 * sub : 128 * sub + 128, 0:128] = attended.astype(jnp.bfloat16)
        around = PR[pl.ds(pl.multiple_of(r0 + 8, 8), 264), :]
        tap = taps[...].astype(jnp.float32)
        filtered = (
            tap[0:1] * around[6:262] + tap[1:2] * around[7:263] + tap[2:3] * around[8:264]
        )
        gate_b = GB[pl.ds(r0, 256), :].astype(jnp.float32)
        AOUT[k, :, 128:256] = (gate_b * filtered).astype(jnp.bfloat16)

    def acopy(k, recv):
        rel = NX - k
        return rc(
            AOUT.at[k], AALL.at[rel], as_.at[k - 1], ar.at[k - 1], dev(dx=k)
        )

    def final(n, mine):
        half = c if mine else 1 - c
        rows = pl.ds(pl.multiple_of(128 * half, 128), 128)
        left = jnp.concatenate(
            [AOUT[0, rows, :], AALL[1, rows, :], AALL[2, rows, :], AALL[3, rows, :]], axis=1
        )
        cols = pl.ds(pl.multiple_of(256 * n, 256), 256)
        right = jnp.concatenate([B3[cols, :], B4[cols, :], B2[cols, :]], axis=1)
        return lax.dot_general(left, right, NT, preferred_element_type=jnp.float32)

    def excopy(n):
        return rc(XS.at[n], XR.at[n], es.at[n], er.at[n], partner)

    PROJ = (0, 1)
    OZY = 2
    OYZ = (3, 4)
    for st in PROJ:
        z_send(st, 0)
        y_send(st, -1)
    for k in range(4):
        oxcopy(k).start()
    for i in range(4):
        t_send(i)
    bias_init()

    def o_step(s):
        z_wait(OZY, s)
        z_send(OZY, s + 1)
        y_send(OZY, s)
        y_fwd(OZY, s - 1)
        if s >= 1:
            y_fin(OZY, s - 2)
        for st in OYZ:
            z_wait(st, s)
            z_send(st, s + 1)

    token_events = {
        0: [], 1: [(t_fwd, 0)], 2: [(t_fwd2, 0), (t_fwd, 1)], 3: [(t_fin, 0), (norm, 0), (t_fwd2, 1)],
        4: [(t_fwd, 2)], 5: [(t_fin, 1), (norm, 1), (t_fwd2, 2)], 6: [(t_fwd, 3), (t_fin, 2), (norm, 2)],
        7: [(t_fwd2, 3)],
    }
    for s in range(8):
        for st in PROJ:
            z_wait(st, s)
            z_send(st, s + 1)
            y_send(st, s)
        for st in PROJ:
            y_fwd(st, s - 1)
            if s >= 1:
                y_fin(st, s - 2)
        for f, i in token_events[s]:
            f(i)
        if s == 1:
            for k in range(4):
                oxcopy(k).wait_recv()
            z_send(OZY, 0)
            y_send(OZY, -1)
            for st in OYZ:
                ay_send(st)
        if s == 2:
            for st in OYZ:
                ay_fwd(st)
        if s == 4:
            for st in OYZ:
                ay_fin(st)
                z_send(st, 0)
    for st in PROJ:
        y_fwd(st, 7)
        y_fin(st, 6)
    o_step(0)
    t_fin(3)
    norm(3)
    for st in PROJ:
        y_fin(st, 7)
    project(3)
    o_step(1)
    project(0)
    halo(0).start()
    halo(1).start()
    project(1)
    o_step(2)
    project(2)
    for k in range(2):
        halo(k).wait_recv()
    PR[8:16, :] = jnp.where(z > 0, PR[8:16, :], 0.0)
    o_step(3)
    mix(2)
    mix(1)
    acopy(2, False).start()
    o_step(4)
    mix(3)
    acopy(1, False).start()
    o_step(5)
    mix(0)
    acopy(3, False).start()
    o_step(6)
    o_step(7)
    y_fwd(OZY, 7)
    y_fin(OZY, 6)
    for k in (2, 1, 3):
        acopy(k, True).wait_recv()
    y_fin(OZY, 7)

    for n in range(8):
        XS[n] = final(n, False).astype(jnp.bfloat16)
        if n >= 1:
            excopy(n - 1).start()
    for n in range(8):
        ACC[n] = final(n, True)
        if n == 0:
            excopy(7).start()
    for n in range(8):
        excopy(n).wait_recv()
        OUTV[:, 256 * n : 256 * n + 256] = (ACC[n] + XR[n].astype(jnp.float32)).astype(jnp.bfloat16)
    store = pltpu.make_async_copy(OUTV, out, osem.at[0])
    store.start()

    for st in (0, 1, 2, 3, 4):
        for s in range(8):
            for way in (0, 1):
                if s < steps(st, way):
                    zcopy(st, way, s, False).wait_send()
    for st in (0, 1, 2):
        for s in range(-1, 8):
            for slot, way, d in slots(st, s):
                for k in range(3):
                    ycopy(st, slot, origin(way, d), k, False).wait_send()
    for st in OYZ:
        for k in range(3):
            aycopy(st, k, False).wait_send()
    for k in range(4):
        oxcopy(k).wait_send()
    for i in range(4):
        for k in range(3):
            tcopy(i, k, False).wait_send()
        for k in range(4):
            dcopy(i, k, False).wait_send()
    for k in range(2):
        halo(k).wait_send()
    for k in (1, 2, 3):
        acopy(k, False).wait_send()
    for n in range(8):
        excopy(n).wait_send()
    store.wait()


def on_device(
    tokens, norm_gain, w_query, w_key, w_value, w_conv_in, w_conv_b, w_conv_c,
    conv_taps, sink_logits, w_attn_out, w_conv_out,
):
    vmem = pl.BlockSpec(memory_space=pltpu.VMEM)
    smem = pl.BlockSpec(memory_space=pltpu.SMEM)
    hbm = pl.BlockSpec(memory_space=pl.ANY)
    bf, f32 = jnp.bfloat16, jnp.float32
    dma = pltpu.SemaphoreType.DMA
    V = pltpu.VMEM
    result = pl.pallas_call(
        kernel,
        out_shape=jax.ShapeDtypeStruct((128, 2048), bf),
        in_specs=[hbm] + [vmem] * 8 + [smem] + [vmem] * 2,
        out_specs=hbm,
        scratch_shapes=[
            V((8, 1024, 256), bf), V((1024, 2048), bf),
            V((2048, 256), bf), V((2048, 384), bf), V((2048, 384), bf), V((2048, 256), bf), V((2048, 384), bf),
            V((1024, 128), bf), V((1152, 128), bf), V((1040, 128), f32), V((1024, 128), bf),
            V((128, 512), f32), V((4, 256, 256), bf), V((4, 256, 256), bf),
            V((8, 128, 256), bf), V((8, 128, 256), bf), V((8, 128, 256), f32), V((128, 2048), bf),
            dma((4,)), dma((1,)),
            dma((5, 2, 8)), dma((5, 2, 8)), dma((3, 17, 3)), dma((3, 17, 3)), dma((2, 3)), dma((2, 3)),
            dma((4, 3)), dma((4, 3)), dma((4, 4)), dma((4, 4)), dma((4,)), dma((4,)),
            dma((2,)), dma((2,)), dma((3,)), dma((3,)), dma((8,)), dma((8,)),
        ],
        compiler_params=pltpu.CompilerParams(
            collective_id=0, has_side_effects=True, vmem_limit_bytes=60 * 1024 * 1024
        ),
    )(
        tokens[0], norm_gain[None], w_query, w_key, w_value, w_conv_in, w_conv_b, w_conv_c,
        conv_taps, sink_logits[None], w_attn_out.T, w_conv_out.T,
    )
    return result[None]


def solution(mesh):
    placed = (
        P("fs", "sp", "tp"),
        P(),
        P(("sp", "fs"), "tp"),
        P(("sp", "fs"), "tp"),
        P(("sp", "fs"), "tp"),
        P(("sp", "fs"), "tp"),
        P(("sp", "fs"), "tp"),
        P(("sp", "fs"), "tp"),
        P(None, "tp"),
        P("tp"),
        P("tp", ("sp", "fs")),
        P("tp", ("sp", "fs")),
    )
    return jax.shard_map(
        on_device,
        mesh=mesh,
        in_specs=placed,
        out_specs=P("fs", ("sp", "tp"), None),
        check_vma=False,
    )
```

time: 407 us -> 99.9 us (0.25)
  waiting for transfers between devices: 342 us -> 0 us
  Pallas kernels: 0 us -> 97.8 us
  matrix products: 30.1 us -> 0 us
  between operations: 13.4 us -> 0.01 us
  other arithmetic: 12 us -> 0 us
  starting transfers between devices: 5.74 us -> 0 us
    all_gather x3 -> x0, waiting for transfers between devices: 292 us -> none  [the longest x1 129 us: in_one_piece(): whole = lax.all_gather(both, axis, axis=dim, tiled=True)]
    pallas_call x0 -> x1, Pallas kernels: none -> 97.8 us  [on_device(): pl.pallas_call(kernel, out_shape=jax.ShapeDtypeStruct((128, 2048), bf), i...]
    reduce_scatter x1 -> x0, waiting for transfers between devices: 49.9 us -> none  [on_device(): lax.psum_scatter((jnp.dot(attended, attn_columns, preferred_element_type=...]
    dot_general x11 -> x0, matrix products: 30.1 us -> none  [the longest x1 11.1 us: on_device(): jnp.dot(conv_out, conv_columns, preferred_element_type=jnp.float32)]
    ppermute x2 -> x0, starting transfers between devices: 5.62 us -> none  [shifted(): return lax.ppermute(block, axis, route)]
    convert_element_type x4 -> x0, other arithmetic: 4.95 us -> none  [the longest x1 2.97 us: norm_rows(): (centred * lax.rsqrt(variance + 1e-05) * norm_gain).astype(jnp.bfloat16)]
    reduce_sum x4 -> x0, other arithmetic: 4.92 us -> none  [the longest x1 2.95 us: norm_rows(): average = jnp.mean(values, axis=-1, keepdims=True)]
  transfers between devices with their start and end apart: 6 -> 0, of which waited for: 4 -> 0; matrix products, arithmetic and copies ran while one was open for 7% -> 0% of each run, Pallas kernels for 0% -> 0%
where the time goes in v1:
time: 99.9 us; the launch traced here: 99.7 us
  Pallas kernels  97.8 us (98%)
  local copies, waits for them, and re-layouts  1.88 us (2%)
    pallas_call x1, Pallas kernels, on_device(): pl.pallas_call(kernel, out_shape=jax.ShapeDtypeStruct((128, 2048), bf), i...  97.8 us

profile of v1, /device:TPU:1, one launch (start us, length us, event | category | flops | bytes accessed | tf_op | source)
XLA Modules:
  0.0 99.7 jit_solution(17714089266011124561)
XLA Ops:
  0.0 97.8 %shard_map.118 = bf16[128,2048]{1,0:T(8,128)(2,1)} custom-call(bf16[1024,256]{1,0:T(8,128)(2,1)} %bitcast.7, f32[1,2048]{1,0:T(1,128)} %bitcast.8, bf16[32,128]{1,0:T(8,128)(2,1)} %wq.1, bf16[32,64]{1,0:T(8,128)(2,1)} %wk.1, bf16[32,64]{1,0:T(8,128)(2,1)} %wv.1, bf16[32,128]{1,0:T(8,128)(2,1)} %wi.1, bf16[32,128]{1,0:T(8,128)(2,1)} %wb.1, ...), custom_call_target="tpu_custom_call" | custom-call | tf_op jit(solution)/shard_map/pallas_call | solution.py:461
  97.8 1.9 %copy.14 = bf16[1,128,2048]{2,1,0:T(8,128)(2,1)} copy(bf16[1,128,2048]{2,1,0:T(8,128)(2,1)} %bitcast.6) | data formatting | bytes 1048576

commit v2 on v1

v2 whole, which is shorter than its diff:
```python
import functools

import jax
import jax.numpy as jnp
from jax import lax
from jax.experimental import pallas as pl
from jax.experimental.pallas import tpu as pltpu
from jax.sharding import PartitionSpec as P

HEADS = 16
HEAD = 64
WINDOW = 128
NZ, NY, NX = 16, 4, 4
MESH = pl.DeviceIdType.MESH
NT = (((1,), (1,)), ((), ()))

STREAMS = (("zy", 256), ("zy", 384), ("zy", 256), ("yz", 256), ("yz", 512))
UP = (8, 7, 8, 7, 8)
SKIP = ((6, 2), (6, 2), (6, 2), (6, 2), (6, 2))
DIRECT = 7
LATE = 96


def kernel(
    tok, gain, wq, wk, wv, wi, wb, wc, taps, sinks, wao, wco,
    out,
    T, N, B0, B1, B2, B3, B4, Q, KV, PR, GB, BIAS, AALL, AOUT, RLY, XS, XR, ACC, OUTV,
    lsem, osem, ss, zr, yr, ayr, tsem, xr, dr, oxr, xlr, hsem, hr, asem, ar, rr, es, er,
):
    z = lax.axis_index("sp")
    y = lax.axis_index("fs")
    t = lax.axis_index("tp")
    x = t // 2
    c = t % 2
    bufs = (B0, B1, B2, B3, B4)

    def dev(dz=0, dy=0, dx=0):
        return (
            lax.rem(z + NZ + dz, NZ),
            lax.rem(y + NY + dy, NY),
            lax.rem(x + NX + dx, NX) * 2 + c,
        )

    partner = (z, y, x * 2 + (1 - c))

    def rc(src, dst, ssem, rsem, to):
        return pltpu.make_async_remote_copy(
            src_ref=src, dst_ref=dst, send_sem=ssem, recv_sem=rsem, device_id=to, device_id_type=MESH
        )

    barrier = pltpu.get_barrier_semaphore()
    peers = [dev(dz=1), dev(dz=-1), dev(dy=1), dev(dy=-1), dev(dx=1), dev(dx=-1), dev(dx=2), partner]
    for peer in peers:
        pl.semaphore_signal(barrier, inc=1, device_id=peer, device_id_type=MESH)

    def tload(i):
        rows = pl.ds(256 * i, 256)
        return pltpu.make_async_copy(tok.at[rows, :], T.at[t, rows, :], lsem.at[i])

    for i in range(4):
        tload(i).start()

    own = pl.ds(pl.multiple_of(32 * (NY * z + y), 32), 32)
    B0[own, 0:128] = wq[...]
    B0[own, 128:256] = jnp.concatenate([wk[...], wv[...]], axis=1)
    B1[own, 0:128] = wi[...]
    B1[own, 128:256] = wb[...]
    B1[own, 256:384] = wc[...]
    B3[own, 0:128] = wao[...]
    B3[own, 128:256] = wco[...]

    pl.semaphore_wait(barrier, len(peers))

    def zblock(st, b):
        buf = bufs[st]
        if STREAMS[st][0] == "zy":
            return buf.at[pl.ds(pl.multiple_of(32 * (NY * b + y), 32), 32), :]
        if st == 4:
            return buf.at[pl.ds(pl.multiple_of(128 * b + LATE, 32), 128 - LATE), :]
        return buf.at[pl.ds(pl.multiple_of(128 * b, 128), 128), :]

    def yblock(st, b, dy):
        yy = lax.rem(y + NY + dy, NY)
        return bufs[st].at[pl.ds(pl.multiple_of(32 * (NY * b + yy), 32), 32), :]

    def steps(st, way):
        return UP[st] if way == 0 else 15 - UP[st]

    def origin(way, s):
        return lax.rem(z + NZ - s, NZ) if way == 0 else lax.rem(z + s, NZ)

    def zarrived(st, way, d):
        ref = zblock(st, origin(way, d))
        return rc(ref, ref, ss.at[st], zr.at[st, way, d - 1], dev(dz=1))

    def zpass(st, d):
        near, jump = SKIP[st]
        for way in (0, 1):
            last = steps(st, way)
            ref = zblock(st, origin(way, d))
            for hops in (1, jump):
                to = d + hops
                if hops == 1 and to > min(near, last) or hops > 1 and (d == 0 or not near < to <= last):
                    continue
                if d <= last:
                    rc(
                        ref, ref, ss.at[st], zr.at[st, way, to - 1], dev(dz=hops if way == 0 else -hops)
                    ).start()

    def zs(st):
        zpass(st, 0)

    def zv(st, d):
        for way in (0, 1):
            if d <= steps(st, way):
                zarrived(st, way, d).wait_recv()
        zpass(st, d)
        if st == 3:
            xl_send(d - 1)

    def slots(st, s):
        if s < 0:
            return [(0, 0, 0)]
        return [(1 + 8 * way + s, way, s + 1) for way in (0, 1) if s < steps(st, way)]

    def ycopy(st, slot, b, d, k, recv):
        if k == 2 and d >= DIRECT:
            ref = yblock(st, b, 2 if recv else 0)
            to = dev(dy=2)
        elif k == 2:
            fwd_up = slot < 9
            if recv:
                ref = yblock(st, b, 2)
            else:
                ref = yblock(st, b, -1 if fwd_up else 1)
            to = dev(dy=1 if fwd_up else -1)
        else:
            ref = yblock(st, b, 0 if not recv else (-1 if k == 0 else 1))
            to = dev(dy=1 if k == 0 else -1)
        return rc(ref, ref, ss.at[st], yr.at[st, slot, k], to)

    def ys(st, e):
        for slot, way, d in slots(st, e - 1):
            for k in (0, 1, 2) if e >= DIRECT else (0, 1):
                ycopy(st, slot, origin(way, d), d, k, False).start()

    def yf(st, e):
        for slot, way, d in slots(st, e - 1):
            b = origin(way, d)
            ycopy(st, slot, b, d, 0 if slot < 9 else 1, True).wait_recv()
            ycopy(st, slot, b, d, 2, False).start()

    def yn(st, e):
        for slot, way, d in slots(st, e - 1):
            b = origin(way, d)
            ycopy(st, slot, b, d, 1 if slot < 9 else 0, True).wait_recv()
            ycopy(st, slot, b, d, 2, True).wait_recv()
            if e >= DIRECT:
                ycopy(st, slot, b, d, 0 if slot < 9 else 1, True).wait_recv()

    def aycopy(st, k, recv):
        up = st % 2 == 0
        if k == 2:
            ref = yblock(st, z, 2) if recv else yblock(st, z, -1 if up else 1)
            to = dev(dy=1 if up else -1)
        else:
            ref = yblock(st, z, 0 if not recv else (-1 if k == 0 else 1))
            to = dev(dy=1 if k == 0 else -1)
        return rc(ref, ref, ss.at[st], ayr.at[st - 3, k], to)

    def ay(st):
        aycopy(st, 0, False).start()
        aycopy(st, 1, False).start()

    def ayf(st):
        aycopy(st, 0 if st % 2 == 0 else 1, True).wait_recv()
        aycopy(st, 2, False).start()

    def aye(st):
        aycopy(st, 1 if st % 2 == 0 else 0, True).wait_recv()
        aycopy(st, 2, True).wait_recv()
        zs(st)

    ox_parts = ((1, 4, 0), (2, 2, 0), (3, 4, 256))

    def oxcopy(k):
        d, st, at = ox_parts[k]
        return rc(B3.at[own, :], bufs[st].at[own, at : at + 256], ss.at[5], oxr.at[k], dev(dx=-d))

    def xlcopy(s, way, k):
        rows = pl.ds(pl.multiple_of(128 * origin(way, s + 1), 128), LATE)
        at = 256 * k
        return rc(
            B3.at[rows, :], B4.at[rows, at : at + 256], ss.at[5 + k], xlr.at[k, way, s], dev(dx=-1 if k == 0 else 1)
        )

    def xl_send(s):
        for way in (0, 1):
            if s < steps(3, way):
                for k in (0, 1):
                    xlcopy(s, way, k).start()

    def xl_wait(s):
        for way in (0, 1):
            if s < steps(3, way):
                for k in (0, 1):
                    xlcopy(s, way, k).wait_recv()

    def tchunk(i, dx, cc):
        tt = lax.rem(x + NX + dx, NX) * 2 + cc
        return T.at[tt, pl.ds(256 * i, 256), :]

    def tcopy(i, k, recv):
        up = i % 2 == 0
        if k == 2:
            ref = tchunk(i, 2, c) if recv else tchunk(i, -1 if up else 1, c)
            to = dev(dx=1 if up else -1)
        else:
            ref = tchunk(i, 0 if not recv else (-1 if k == 0 else 1), c)
            to = dev(dx=1 if k == 0 else -1)
        return rc(ref, ref, tsem.at[0], xr.at[i, k], to)

    def dcopy(i, k, recv):
        ref = tchunk(i, (0, -1, 1, 2)[k], c if not recv else 1 - c)
        return rc(ref, ref, tsem.at[0], dr.at[i, k], partner)

    def ts(i):
        tload(i).wait()
        tcopy(i, 0, False).start()
        tcopy(i, 1, False).start()
        dcopy(i, 0, False).start()

    def tf(i):
        first = i % 2
        tcopy(i, first, True).wait_recv()
        tcopy(i, 2, False).start()
        dcopy(i, 1 + first, False).start()

    def tg(i):
        first = i % 2
        tcopy(i, 1 - first, True).wait_recv()
        dcopy(i, 2 - first, False).start()

    def th(i):
        tcopy(i, 2, True).wait_recv()
        dcopy(i, 3, False).start()

    def td(i):
        for k in range(4):
            dcopy(i, k, True).wait_recv()

    def norm(i, h):
        base = 256 * i + 64 * h

        @pl.loop(0, 2)
        def _(j):
            rows = [pl.ds(pl.multiple_of(base + 32 * j + 16 * g, 16), 16) for g in range(2)]
            averages, scales = [], []
            for r in rows:
                total = T[0, r, :].astype(jnp.float32)
                for k in range(1, 8):
                    total += T[k, r, :].astype(jnp.float32)
                averages.append(jnp.sum(total, axis=1, keepdims=True) * (1.0 / 2048))
            for r, average in zip(rows, averages):
                squares = None
                for k in range(8):
                    centred = T[k, r, :].astype(jnp.float32) - average
                    squares = centred * centred if k == 0 else squares + centred * centred
                variance = jnp.sum(squares, axis=1, keepdims=True) * (1.0 / 2048)
                scales.append(lax.rsqrt(variance + 1e-05))
            for k in range(8):
                cols = slice(256 * k, 256 * k + 256)
                for r, average, scale in zip(rows, averages, scales):
                    centred = T[k, r, :].astype(jnp.float32) - average
                    N[r, cols] = (centred * scale * gain[:, cols]).astype(jnp.bfloat16)

    def proj(i):
        rows = slice(256 * i, 256 * i + 256)
        normed = N[rows, :]
        qkv = jnp.dot(normed, B0[...], preferred_element_type=jnp.float32)
        Q[rows, :] = qkv[:, 0:128].astype(jnp.bfloat16)
        KV[128 + 256 * i : 128 + 256 * i + 256, :] = qkv[:, 128:256].astype(jnp.bfloat16)
        ibc = jnp.dot(normed, B1[...], preferred_element_type=jnp.float32).astype(jnp.bfloat16)
        inner = ibc[:, 0:128].astype(jnp.float32)
        gate_c = ibc[:, 256:384].astype(jnp.float32)
        product = (gate_c * inner).astype(jnp.bfloat16)
        PR[16 + 256 * i : 16 + 256 * i + 256, :] = product.astype(jnp.float32)
        GB[rows, :] = ibc[:, 128:256]

    def halo(k):
        to = dev(dz=1)
        if k == 0:
            return rc(KV.at[1024:1152, :], KV.at[0:128, :], hsem.at[0], hr.at[0], to)
        return rc(PR.at[1032:1040, :], PR.at[8:16, :], hsem.at[1], hr.at[1], to)

    def bias_init():
        row = lax.broadcasted_iota(jnp.int32, (128, 512), 0)
        col = lax.broadcasted_iota(jnp.int32, (128, 512), 1)
        upper = col >= 256
        distance = 128 + row - jnp.where(upper, col - 256, col)
        head = jnp.where(upper, 1, 0) + 2 * t
        slope = jnp.exp2((head + 1).astype(jnp.float32) * (-8.0 / HEADS))
        keep = (distance >= 0) & (distance < WINDOW)
        BIAS[...] = jnp.where(keep, -slope * distance.astype(jnp.float32), -jnp.inf)

    def mix(k, u):
        q0 = pl.multiple_of(256 * lax.rem(x + k, NX) + 128 * u, 128)
        lane = lax.broadcasted_iota(jnp.int32, (256, 128), 1)
        low = lane < 64
        q = Q[pl.ds(q0, 128), :]
        kv = KV[pl.ds(q0, 256), :].astype(jnp.float32)
        vk = pltpu.roll(kv, 64, 1)
        keys = jnp.concatenate(
            [jnp.where(low, kv, 0.0), jnp.where(low, 0.0, vk)], axis=0
        ).astype(jnp.bfloat16)
        values = jnp.concatenate(
            [jnp.where(low, vk, 0.0), jnp.where(low, 0.0, kv)], axis=0
        ).astype(jnp.bfloat16)
        scores = lax.dot_general(q, keys, NT, preferred_element_type=jnp.float32)
        scores = scores * HEAD ** (-0.5) + BIAS[...]
        if u == 0:
            col = lax.broadcasted_iota(jnp.int32, (128, 512), 1)
            place = jnp.bitwise_and(col, 255) + (1024 * z + q0 - WINDOW)
            scores = jnp.where(place >= 0, scores, -jnp.inf)
        weights = []
        for g in range(2):
            part = scores[:, 256 * g : 256 * g + 256]
            sink = sinks[0, g]
            top = jnp.maximum(jnp.max(part, axis=1, keepdims=True), sink)
            raised = jnp.exp(part - top)
            below = jnp.sum(raised, axis=1, keepdims=True) + jnp.exp(sink - top)
            weights.append((raised * (1.0 / below)).astype(jnp.bfloat16))
        attended = jnp.dot(
            jnp.concatenate(weights, axis=1), values, preferred_element_type=jnp.float32
        )
        half = slice(128 * u, 128 * u + 128)
        AOUT[k, half, 0:128] = attended.astype(jnp.bfloat16)
        around = PR[pl.ds(pl.multiple_of(q0 + 8, 8), 136), :]
        tap = taps[...].astype(jnp.float32)
        filtered = (
            tap[0:1] * around[6:134] + tap[1:2] * around[7:135] + tap[2:3] * around[8:136]
        )
        gate_b = GB[pl.ds(q0, 128), :].astype(jnp.float32)
        AOUT[k, half, 128:256] = (gate_b * filtered).astype(jnp.bfloat16)

    def acopy(k, u):
        half = pl.ds(128 * u, 128)
        if k == 2:
            return rc(AOUT.at[k, half, :], RLY.at[u], asem.at[0], rr.at[u], dev(dx=1 - 2 * u))
        return rc(AOUT.at[k, half, :], AALL.at[NX - k, half, :], asem.at[0], ar.at[k - 1, u], dev(dx=k))

    def relay(u):
        half = pl.ds(128 * u, 128)
        return rc(RLY.at[u], AALL.at[2, half, :], asem.at[1], ar.at[1, u], dev(dx=1 - 2 * u))

    def out_dot(left, buf, n, at):
        right = buf[512 * n : 512 * n + 512, at : at + 256]
        return lax.dot_general(left, right, NT, preferred_element_type=jnp.float32)

    def excopy(n):
        return rc(XS.at[n], XR.at[n], es.at[0], er.at[n], partner)

    def store(n):
        cols = slice(512 * n, 512 * n + 512)
        return pltpu.make_async_copy(OUTV.at[:, cols], out.at[:, cols], osem.at[n])

    def start():
        bias_init()

    def ox():
        for k in range(3):
            oxcopy(k).start()

    def oxw():
        for k in range(3):
            oxcopy(k).wait_recv()

    def xw(d):
        xl_wait(d - 1)

    def hs():
        halo(0).start()
        halo(1).start()

    def hw():
        halo(0).wait_recv()
        halo(1).wait_recv()
        PR[8:16, :] = jnp.where(z > 0, PR[8:16, :], 0.0)

    def asend(k, u):
        acopy(k, u).start()

    def af(u):
        acopy(2, u).wait_recv()
        relay(u).start()

    def aw(k):
        for u in (0, 1):
            (relay(u) if k == 2 else acopy(k, u)).wait_recv()

    def f0():
        for n in range(4):
            ACC[:, 512 * n : 512 * n + 512] = out_dot(AOUT[0], B3, n, 0)

    def f1():
        for n in range(4):
            ACC[:, 512 * n : 512 * n + 512] += out_dot(AALL[1], B4, n, 0)

    def f3():
        for n in range(4):
            ACC[:, 512 * n : 512 * n + 512] += out_dot(AALL[3], B4, n, 256)

    def ft():
        rows = pl.ds(pl.multiple_of(128 * (1 - c), 128), 128)
        for n in range(4):
            total = ACC[rows, 512 * n : 512 * n + 512] + out_dot(AALL[2, rows, :], B2, n, 0)
            XS[n] = total.astype(jnp.bfloat16)
            if n >= 1:
                excopy(n - 1).start()

    def fo():
        rows = pl.ds(pl.multiple_of(128 * c, 128), 128)
        for n in range(4):
            cols = slice(512 * n, 512 * n + 512)
            ACC[rows, cols] += out_dot(AALL[2, rows, :], B2, n, 0)
            if n == 0:
                excopy(3).start()

    def comb():
        rows = pl.ds(pl.multiple_of(128 * c, 128), 128)
        for n in range(4):
            cols = slice(512 * n, 512 * n + 512)
            excopy(n).wait_recv()
            OUTV[:, cols] = (ACC[rows, cols] + XR[n].astype(jnp.float32)).astype(jnp.bfloat16)
            if n >= 1:
                store(n - 1).start()

    order = (
        (start,), (zs, 1), (zs, 0), (ox,), (ay, 3), (ys, 0, 0), (ys, 1, 0), (ts, 3), (ts, 0), (ts, 2), (ts, 1),
        (ayf, 3), (zv, 1, 1), (ys, 1, 1), (yf, 0, 0), (zv, 0, 1), (ys, 0, 1), (yf, 1, 0), (oxw,), (ay, 4), (tg, 3),
        (aye, 3), (zv, 1, 2), (ys, 1, 2), (tf, 3), (zv, 0, 2), (ys, 0, 2), (yf, 1, 1), (yn, 0, 0), (yf, 0, 1),
        (yn, 1, 0), (tf, 0), (ayf, 4), (tg, 0), (yf, 1, 2), (zv, 3, 1), (zv, 1, 3), (ys, 1, 3), (yf, 0, 2),
        (zv, 0, 3), (zs, 2), (ys, 0, 3), (ys, 2, 0), (tf, 2), (yn, 1, 1), (yn, 0, 1), (tg, 2), (aye, 4), (yn, 1, 2),
        (zv, 3, 2), (tg, 1), (yf, 1, 3), (zv, 1, 4), (ys, 1, 4), (yn, 0, 2), (tf, 1), (zv, 0, 4), (ys, 0, 4),
        (yf, 0, 3), (yf, 2, 0), (zv, 4, 1), (th, 0), (yn, 1, 3), (th, 3), (zv, 3, 3), (td, 0), (yf, 1, 4),
        (norm, 0, 0), (zv, 1, 5), (ys, 1, 5), (norm, 0, 2), (zv, 0, 5), (zv, 2, 1), (ys, 0, 5), (ys, 2, 1),
        (norm, 0, 1), (yf, 0, 4), (td, 3), (norm, 3, 0), (yn, 0, 3), (norm, 3, 2), (zv, 4, 2), (xw, 1), (norm, 3, 1),
        (yn, 2, 0), (norm, 3, 3), (norm, 0, 3), (yn, 1, 4), (th, 2), (zv, 3, 4), (zv, 1, 6), (ys, 1, 6), (yf, 1, 5),
        (td, 2), (norm, 2, 0), (yf, 0, 5), (norm, 2, 2), (norm, 2, 1), (xw, 2), (zv, 0, 6), (ys, 0, 6), (yf, 2, 1),
        (norm, 2, 3), (zv, 1, 7), (ys, 1, 7), (yn, 0, 4), (th, 1), (zv, 0, 7), (zv, 2, 2), (ys, 0, 7), (ys, 2, 2),
        (zv, 4, 3), (td, 1), (norm, 1, 2), (norm, 1, 1), (yf, 1, 6), (norm, 1, 3), (xw, 3), (norm, 1, 0), (yn, 1, 5),
        (zv, 3, 5), (yn, 0, 5), (yf, 0, 6), (yn, 2, 1), (zv, 0, 8), (ys, 0, 8), (zv, 2, 3), (ys, 2, 3), (zv, 1, 8),
        (ys, 1, 8), (xw, 4), (zv, 4, 4), (yn, 1, 7), (zv, 3, 6), (xw, 5), (yn, 0, 7), (yf, 2, 2), (yn, 1, 6),
        (yn, 0, 6), (zv, 3, 7), (zv, 2, 4), (ys, 2, 4), (yf, 2, 3), (yn, 0, 8), (zv, 4, 5), (xw, 6), (yn, 2, 2),
        (yn, 1, 8), (proj, 3), (hs,), (proj, 1), (zv, 3, 8), (zv, 2, 5), (yf, 2, 4), (ys, 2, 5), (yn, 2, 3),
        (proj, 0), (zv, 4, 6), (proj, 2), (xw, 7), (zv, 4, 7), (hw,), (mix, 2, 1), (asend, 2, 1), (mix, 2, 0),
        (zv, 2, 6), (ys, 2, 6), (asend, 2, 0), (yn, 2, 4), (mix, 1, 0), (yf, 2, 5), (asend, 1, 0), (mix, 1, 1),
        (zv, 2, 7), (ys, 2, 7), (asend, 1, 1), (mix, 3, 1), (asend, 3, 1), (mix, 3, 0), (asend, 3, 0), (mix, 0, 1),
        (zv, 4, 8), (mix, 0, 0), (xw, 8), (f0,), (yf, 2, 6), (af, 1), (yn, 2, 5), (zv, 2, 8), (ys, 2, 8), (af, 0),
        (yn, 2, 7), (yn, 2, 6), (aw, 1), (aw, 3), (f1,), (f3,), (yn, 2, 8), (aw, 2), (ft,), (fo,), (comb,),
    )
    for event, *where in order:
        with jax.named_scope(event.__name__ + "_".join(map(str, where))):
            event(*where)
    store(3).start()

    def sent(ref, sem):
        pltpu.make_async_copy(ref, ref, sem).wait()

    for st in (0, 1, 2):
        sent(bufs[st].at[0:2016, :], ss.at[st])
    sent(B3.at[0:2016, :], ss.at[3])
    sent(B4.at[0 : 96 + 15 * (128 - LATE), :], ss.at[4])
    sent(B3.at[0 : 96 + 15 * LATE, :], ss.at[5])
    sent(B3.at[0 : 15 * LATE, :], ss.at[6])
    sent(T.at[0:7], tsem.at[0])
    for k in range(2):
        halo(k).wait_send()
    sent(AOUT.at[0:3], asem.at[0])
    sent(RLY, asem.at[1])
    sent(XS, es.at[0])
    for n in range(4):
        store(n).wait()


def on_device(
    tokens, norm_gain, w_query, w_key, w_value, w_conv_in, w_conv_b, w_conv_c,
    conv_taps, sink_logits, w_attn_out, w_conv_out,
):
    vmem = pl.BlockSpec(memory_space=pltpu.VMEM)
    smem = pl.BlockSpec(memory_space=pltpu.SMEM)
    hbm = pl.BlockSpec(memory_space=pl.ANY)
    bf, f32 = jnp.bfloat16, jnp.float32
    dma = pltpu.SemaphoreType.DMA
    V = pltpu.VMEM
    result = pl.pallas_call(
        kernel,
        out_shape=jax.ShapeDtypeStruct((128, 2048), bf),
        in_specs=[hbm] + [vmem] * 8 + [smem] + [vmem] * 2,
        out_specs=hbm,
        scratch_shapes=[
            V((8, 1024, 256), bf), V((1024, 2048), bf),
            V((2048, 256), bf), V((2048, 384), bf), V((2048, 256), bf), V((2048, 256), bf), V((2048, 512), bf),
            V((1024, 128), bf), V((1152, 128), bf), V((1040, 128), f32), V((1024, 128), bf),
            V((128, 512), f32), V((4, 256, 256), bf), V((4, 256, 256), bf), V((2, 128, 256), bf),
            V((4, 128, 512), bf), V((4, 128, 512), bf), V((256, 2048), f32), V((128, 2048), bf),
            dma((4,)), dma((4,)),
            dma((7,)), dma((5, 2, 8)), dma((3, 17, 3)), dma((2, 3)),
            dma((1,)), dma((4, 3)), dma((4, 4)), dma((3,)), dma((2, 2, 8)),
            dma((2,)), dma((2,)), dma((2,)), dma((3, 2)), dma((2,)), dma((1,)), dma((4,)),
        ],
        compiler_params=pltpu.CompilerParams(
            collective_id=0, has_side_effects=True, vmem_limit_bytes=60 * 1024 * 1024
        ),
    )(
        tokens[0], norm_gain[None], w_query, w_key, w_value, w_conv_in, w_conv_b, w_conv_c,
        conv_taps, sink_logits[None], w_attn_out.T, w_conv_out.T,
    )
    return result[None]


def solution(mesh):
    placed = (
        P("fs", "sp", "tp"),
        P(),
        P(("sp", "fs"), "tp"),
        P(("sp", "fs"), "tp"),
        P(("sp", "fs"), "tp"),
        P(("sp", "fs"), "tp"),
        P(("sp", "fs"), "tp"),
        P(("sp", "fs"), "tp"),
        P(None, "tp"),
        P("tp"),
        P("tp", ("sp", "fs")),
        P("tp", ("sp", "fs")),
    )
    return jax.shard_map(
        on_device,
        mesh=mesh,
        in_specs=placed,
        out_specs=P("fs", ("sp", "tp"), None),
        check_vma=False,
    )
```

time: 99.9 us -> 77.1 us (0.77)
  Pallas kernels: 97.8 us -> 75.1 us
    pallas_call x1, Pallas kernels: 97.8 us -> 75.1 us  [on_device(): pl.pallas_call(kernel, out_shape=jax.ShapeDtypeStruct((128, 2048), bf), i...]
where the time goes in v2:
time: 77.1 us; the launch traced here: 76.9 us
  Pallas kernels  75.1 us (97%)
  local copies, waits for them, and re-layouts  1.88 us (2%)
    pallas_call x1, Pallas kernels, on_device(): pl.pallas_call(kernel, out_shape=jax.ShapeDtypeStruct((128, 2048), bf), i...  75.1 us
    unnamed x1, local copies, waits for them, and re-layouts  1.88 us

profile of v2, /device:TPU:1, one launch (start us, length us, event | category | flops | bytes accessed | tf_op | source)
XLA Modules:
  0.0 76.9 jit_solution(16017740720771828263)
XLA Ops:
  0.0 75.1 %shard_map.118 = bf16[128,2048]{1,0:T(8,128)(2,1)} custom-call(bf16[1024,256]{1,0:T(8,128)(2,1)} %bitcast.7, f32[1,2048]{1,0:T(1,128)} %bitcast.8, bf16[32,128]{1,0:T(8,128)(2,1)} %wq.1, bf16[32,64]{1,0:T(8,128)(2,1)} %wk.1, bf16[32,64]{1,0:T(8,128)(2,1)} %wv.1, bf16[32,128]{1,0:T(8,128)(2,1)} %wi.1, bf16[32,128]{1,0:T(8,128)(2,1)} %wb.1, ...), custom_call_target="tpu_custom_call" | custom-call | tf_op jit(solution)/shard_map/pallas_call | solution.py:496
  75.1 1.9 %copy.14 = bf16[1,128,2048]{2,1,0:T(8,128)(2,1)} copy(bf16[1,128,2048]{2,1,0:T(8,128)(2,1)} %bitcast.6) | data formatting | bytes 1048576

commit v3 on v2

--- a/solution.py
+++ b/solution.py
@@ -19,12 +19,13 @@
 SKIP = ((6, 2), (6, 2), (6, 2), (6, 2), (6, 2))
 DIRECT = 7
 LATE = 96
+EARLY = 4
 
 
 def kernel(
     tok, gain, wq, wk, wv, wi, wb, wc, taps, sinks, wao, wco,
     out,
-    T, N, B0, B1, B2, B3, B4, Q, KV, PR, GB, BIAS, AALL, AOUT, RLY, XS, XR, ACC, OUTV,
+    T, N, B0, B1, B2, B3, B4, Q, KV, PR, GB, BIAS, AALL, AOUT, RLY, XS, XR, ACC, OUTV, PACC,
     lsem, osem, ss, zr, yr, ayr, tsem, xr, dr, oxr, xlr, hsem, hr, asem, ar, rr, es, er,
 ):
     z = lax.axis_index("sp")
@@ -58,7 +59,8 @@
         return pltpu.make_async_copy(tok.at[rows, :], T.at[t, rows, :], lsem.at[i])
 
     for i in range(4):
-        tload(i).start()
+        with jax.named_scope("load"):
+            tload(i).start()
 
     own = pl.ds(pl.multiple_of(32 * (NY * z + y), 32), 32)
     B0[own, 0:128] = wq[...]
@@ -69,14 +71,15 @@
     B3[own, 0:128] = wao[...]
     B3[own, 128:256] = wco[...]
 
-    pl.semaphore_wait(barrier, len(peers))
+    with jax.named_scope("barrier"):
+        pl.semaphore_wait(barrier, len(peers))
 
     def zblock(st, b):
         buf = bufs[st]
         if STREAMS[st][0] == "zy":
             return buf.at[pl.ds(pl.multiple_of(32 * (NY * b + y), 32), 32), :]
         if st == 4:
-            return buf.at[pl.ds(pl.multiple_of(128 * b + LATE, 32), 128 - LATE), :]
+            return buf.at[pl.ds(pl.multiple_of(128 * b + LATE, 16), 128 - LATE), :]
         return buf.at[pl.ds(pl.multiple_of(128 * b, 128), 128), :]
 
     def yblock(st, b, dy):
@@ -274,13 +277,35 @@
                     centred = T[k, r, :].astype(jnp.float32) - average
                     N[r, cols] = (centred * scale * gain[:, cols]).astype(jnp.bfloat16)
 
+    def part(i, pairs):
+        rows = slice(256 * i, 256 * i + 256)
+        qkv = ibc = None
+        for d, e in pairs:
+            one = pl.multiple_of(128 * origin(0, d), 128)
+            two = pl.multiple_of(128 * origin(0 if d == 0 else 1, e), 128)
+            left = jnp.concatenate([N[rows, pl.ds(one, 128)], N[rows, pl.ds(two, 128)]], axis=1)
+            for buf in (B0, B1):
+                right = jnp.concatenate([buf[pl.ds(one, 128), :], buf[pl.ds(two, 128), :]], axis=0)
+                term = jnp.dot(left, right, preferred_element_type=jnp.float32)
+                if buf is B0:
+                    qkv = term if qkv is None else qkv + term
+                else:
+                    ibc = term if ibc is None else ibc + term
+        return qkv, ibc
+
+    def pe(i):
+        rows = slice(256 * i, 256 * i + 256)
+        qkv, ibc = part(i, [(d, d) for d in range(1, EARLY + 1)])
+        PACC[rows, 0:256] = qkv
+        PACC[rows, 256:640] = ibc
+
     def proj(i):
         rows = slice(256 * i, 256 * i + 256)
-        normed = N[rows, :]
-        qkv = jnp.dot(normed, B0[...], preferred_element_type=jnp.float32)
-        Q[rows, :] = qkv[:, 0:128].astype(jnp.bfloat16)
-        KV[128 + 256 * i : 128 + 256 * i + 256, :] = qkv[:, 128:256].astype(jnp.bfloat16)
-        ibc = jnp.dot(normed, B1[...], preferred_element_type=jnp.float32).astype(jnp.bfloat16)
+        qkv, ibc = part(i, [(d, d) for d in range(EARLY + 1, 8)] + [(0, 8)])
+        qkv = (qkv + PACC[rows, 0:256]).astype(jnp.bfloat16)
+        ibc = (ibc + PACC[rows, 256:640]).astype(jnp.bfloat16)
+        Q[rows, :] = qkv[:, 0:128]
+        KV[128 + 256 * i : 128 + 256 * i + 256, :] = qkv[:, 128:256]
         inner = ibc[:, 0:128].astype(jnp.float32)
         gate_c = ibc[:, 256:384].astype(jnp.float32)
         product = (gate_c * inner).astype(jnp.bfloat16)
@@ -303,7 +328,11 @@
         keep = (distance >= 0) & (distance < WINDOW)
         BIAS[...] = jnp.where(keep, -slope * distance.astype(jnp.float32), -jnp.inf)
 
-    def mix(k, u):
+    def mix(k):
+        for u in (0, 1):
+            mix_half(k, u)
+
+    def mix_half(k, u):
         q0 = pl.multiple_of(256 * lax.rem(x + k, NX) + 128 * u, 128)
         lane = lax.broadcasted_iota(jnp.int32, (256, 128), 1)
         low = lane < 64
@@ -387,8 +416,9 @@
         halo(1).wait_recv()
         PR[8:16, :] = jnp.where(z > 0, PR[8:16, :], 0.0)
 
-    def asend(k, u):
-        acopy(k, u).start()
+    def asend(k):
+        for u in (0, 1):
+            acopy(k, u).start()
 
     def af(u):
         acopy(2, u).wait_recv()
@@ -436,51 +466,53 @@
                 store(n - 1).start()
 
     order = (
-        (start,), (zs, 1), (zs, 0), (ox,), (ay, 3), (ys, 0, 0), (ys, 1, 0), (ts, 3), (ts, 0), (ts, 2), (ts, 1),
-        (ayf, 3), (zv, 1, 1), (ys, 1, 1), (yf, 0, 0), (zv, 0, 1), (ys, 0, 1), (yf, 1, 0), (oxw,), (ay, 4), (tg, 3),
-        (aye, 3), (zv, 1, 2), (ys, 1, 2), (tf, 3), (zv, 0, 2), (ys, 0, 2), (yf, 1, 1), (yn, 0, 0), (yf, 0, 1),
-        (yn, 1, 0), (tf, 0), (ayf, 4), (tg, 0), (yf, 1, 2), (zv, 3, 1), (zv, 1, 3), (ys, 1, 3), (yf, 0, 2),
-        (zv, 0, 3), (zs, 2), (ys, 0, 3), (ys, 2, 0), (tf, 2), (yn, 1, 1), (yn, 0, 1), (tg, 2), (aye, 4), (yn, 1, 2),
-        (zv, 3, 2), (tg, 1), (yf, 1, 3), (zv, 1, 4), (ys, 1, 4), (yn, 0, 2), (tf, 1), (zv, 0, 4), (ys, 0, 4),
-        (yf, 0, 3), (yf, 2, 0), (zv, 4, 1), (th, 0), (yn, 1, 3), (th, 3), (zv, 3, 3), (td, 0), (yf, 1, 4),
-        (norm, 0, 0), (zv, 1, 5), (ys, 1, 5), (norm, 0, 2), (zv, 0, 5), (zv, 2, 1), (ys, 0, 5), (ys, 2, 1),
-        (norm, 0, 1), (yf, 0, 4), (td, 3), (norm, 3, 0), (yn, 0, 3), (norm, 3, 2), (zv, 4, 2), (xw, 1), (norm, 3, 1),
-        (yn, 2, 0), (norm, 3, 3), (norm, 0, 3), (yn, 1, 4), (th, 2), (zv, 3, 4), (zv, 1, 6), (ys, 1, 6), (yf, 1, 5),
-        (td, 2), (norm, 2, 0), (yf, 0, 5), (norm, 2, 2), (norm, 2, 1), (xw, 2), (zv, 0, 6), (ys, 0, 6), (yf, 2, 1),
-        (norm, 2, 3), (zv, 1, 7), (ys, 1, 7), (yn, 0, 4), (th, 1), (zv, 0, 7), (zv, 2, 2), (ys, 0, 7), (ys, 2, 2),
-        (zv, 4, 3), (td, 1), (norm, 1, 2), (norm, 1, 1), (yf, 1, 6), (norm, 1, 3), (xw, 3), (norm, 1, 0), (yn, 1, 5),
-        (zv, 3, 5), (yn, 0, 5), (yf, 0, 6), (yn, 2, 1), (zv, 0, 8), (ys, 0, 8), (zv, 2, 3), (ys, 2, 3), (zv, 1, 8),
-        (ys, 1, 8), (xw, 4), (zv, 4, 4), (yn, 1, 7), (zv, 3, 6), (xw, 5), (yn, 0, 7), (yf, 2, 2), (yn, 1, 6),
-        (yn, 0, 6), (zv, 3, 7), (zv, 2, 4), (ys, 2, 4), (yf, 2, 3), (yn, 0, 8), (zv, 4, 5), (xw, 6), (yn, 2, 2),
-        (yn, 1, 8), (proj, 3), (hs,), (proj, 1), (zv, 3, 8), (zv, 2, 5), (yf, 2, 4), (ys, 2, 5), (yn, 2, 3),
-        (proj, 0), (zv, 4, 6), (proj, 2), (xw, 7), (zv, 4, 7), (hw,), (mix, 2, 1), (asend, 2, 1), (mix, 2, 0),
-        (zv, 2, 6), (ys, 2, 6), (asend, 2, 0), (yn, 2, 4), (mix, 1, 0), (yf, 2, 5), (asend, 1, 0), (mix, 1, 1),
-        (zv, 2, 7), (ys, 2, 7), (asend, 1, 1), (mix, 3, 1), (asend, 3, 1), (mix, 3, 0), (asend, 3, 0), (mix, 0, 1),
-        (zv, 4, 8), (mix, 0, 0), (xw, 8), (f0,), (yf, 2, 6), (af, 1), (yn, 2, 5), (zv, 2, 8), (ys, 2, 8), (af, 0),
-        (yn, 2, 7), (yn, 2, 6), (aw, 1), (aw, 3), (f1,), (f3,), (yn, 2, 8), (aw, 2), (ft,), (fo,), (comb,),
+        (start,), (zs, 0), (ox,), (ts, 1), (ay, 3), (zs, 1), (ys, 0, 0), (ys, 1, 0), (zv, 0, 1), (oxw,), (ts, 0),
+        (zs, 2), (ay, 4), (ayf, 3), (zv, 1, 1), (ts, 3), (zv, 0, 2), (ayf, 4), (ts, 2), (zv, 2, 1), (ys, 1, 1),
+        (zv, 1, 2), (aye, 3), (zv, 0, 3), (tg, 0), (yf, 1, 0), (aye, 4), (tf, 0), (ys, 1, 2), (ys, 0, 3), (zv, 1, 3),
+        (ys, 0, 2), (zv, 2, 2), (tf, 3), (tg, 3), (ys, 1, 3), (zv, 0, 4), (zv, 3, 1), (ys, 0, 1), (yf, 1, 2),
+        (zv, 4, 1), (yf, 1, 1), (zv, 1, 4), (zv, 2, 3), (ys, 1, 4), (yf, 0, 3), (zv, 0, 5), (ys, 0, 5), (tf, 2),
+        (tf, 1), (th, 3), (ys, 0, 4), (zv, 3, 2), (th, 0), (ys, 2, 0), (yn, 1, 2), (yf, 0, 2), (yf, 0, 0), (ys, 2, 3),
+        (zv, 4, 2), (zv, 2, 4), (zv, 1, 5), (yf, 1, 3), (ys, 1, 5), (yf, 0, 4), (td, 3), (yf, 0, 1), (ys, 2, 4),
+        (tg, 2), (yf, 0, 5), (norm, 3, 2), (yf, 1, 4), (th, 2), (yn, 0, 3), (zv, 3, 3), (zv, 0, 6), (zv, 0, 7),
+        (ys, 0, 6), (norm, 3, 3), (norm, 3, 0), (yn, 0, 0), (th, 1), (tg, 1), (zv, 2, 5), (yn, 1, 1), (ys, 0, 7),
+        (td, 2), (norm, 2, 0), (norm, 2, 3), (zv, 1, 6), (zv, 4, 3), (td, 0), (ys, 1, 6), (td, 1), (norm, 1, 1),
+        (yf, 1, 5), (yn, 0, 5), (zv, 1, 7), (yn, 0, 1), (yn, 1, 3), (ys, 1, 7), (zv, 3, 4), (yn, 0, 2), (yn, 1, 4),
+        (norm, 1, 0), (norm, 0, 1), (yn, 0, 4), (norm, 0, 3), (xw, 1), (zv, 0, 8), (norm, 3, 1), (norm, 0, 0),
+        (yf, 0, 6), (zv, 2, 6), (ys, 0, 8), (xw, 3), (norm, 0, 2), (yf, 1, 6), (norm, 1, 3), (zv, 2, 7), (zv, 4, 4),
+        (yn, 1, 0), (zv, 1, 8), (yn, 0, 7), (ys, 1, 8), (zv, 3, 5), (norm, 1, 2), (pe, 1), (norm, 2, 1), (yn, 1, 5),
+        (pe, 3), (xw, 4), (yf, 2, 4), (ys, 2, 1), (norm, 2, 2), (ys, 2, 6), (pe, 0), (yn, 1, 6), (yn, 1, 7),
+        (yn, 0, 8), (yf, 2, 3), (yn, 0, 6), (yn, 1, 8), (proj, 3), (ys, 2, 5), (hs,), (zv, 3, 6), (pe, 2), (ys, 2, 2),
+        (ys, 2, 7), (proj, 0), (proj, 2), (proj, 1), (yn, 2, 3), (xw, 5), (zv, 4, 5), (zv, 3, 7), (zv, 2, 8), (hw,),
+        (mix, 2), (asend, 2), (yf, 2, 5), (mix, 3), (asend, 3), (mix, 1), (asend, 1), (yf, 2, 0), (yf, 2, 6),
+        (yf, 2, 1), (yn, 2, 4), (mix, 0), (ys, 2, 8), (zv, 3, 8), (zv, 4, 6), (xw, 7), (yn, 2, 5), (f0,), (yf, 2, 2),
+        (xw, 2), (af, 0), (xw, 6), (af, 1), (aw, 3), (yn, 2, 2), (yn, 2, 1), (yn, 2, 6), (aw, 1), (yn, 2, 7),
+        (zv, 4, 8), (zv, 4, 7), (yn, 2, 8), (yn, 2, 0), (xw, 8), (f1,), (f3,), (aw, 2), (ft,), (fo,), (comb,),
     )
     for event, *where in order:
         with jax.named_scope(event.__name__ + "_".join(map(str, where))):
             event(*where)
-    store(3).start()
+    with jax.named_scope("tail"):
+        store(3).start()
 
     def sent(ref, sem):
         pltpu.make_async_copy(ref, ref, sem).wait()
 
-    for st in (0, 1, 2):
-        sent(bufs[st].at[0:2016, :], ss.at[st])
-    sent(B3.at[0:2016, :], ss.at[3])
-    sent(B4.at[0 : 96 + 15 * (128 - LATE), :], ss.at[4])
-    sent(B3.at[0 : 96 + 15 * LATE, :], ss.at[5])
-    sent(B3.at[0 : 15 * LATE, :], ss.at[6])
-    sent(T.at[0:7], tsem.at[0])
-    for k in range(2):
-        halo(k).wait_send()
-    sent(AOUT.at[0:3], asem.at[0])
-    sent(RLY, asem.at[1])
-    sent(XS, es.at[0])
-    for n in range(4):
-        store(n).wait()
+    with jax.named_scope("sent"):
+        for st in (0, 1, 2):
+            sent(bufs[st].at[0:2016, :], ss.at[st])
+        sent(B3.at[0:2016, :], ss.at[3])
+        sent(B4.at[0 : 96 + 15 * (128 - LATE), :], ss.at[4])
+        sent(B3.at[0 : 96 + 15 * LATE, :], ss.at[5])
+        sent(B3.at[0 : 15 * LATE, :], ss.at[6])
+        sent(T.at[0:7], tsem.at[0])
+        for k in range(2):
+            halo(k).wait_send()
+        sent(AOUT.at[0:3], asem.at[0])
+        sent(RLY, asem.at[1])
+        sent(XS, es.at[0])
+    with jax.named_scope("stored"):
+        for n in range(4):
+            store(n).wait()
 
 
 def on_device(
@@ -503,7 +535,7 @@
             V((2048, 256), bf), V((2048, 384), bf), V((2048, 256), bf), V((2048, 256), bf), V((2048, 512), bf),
             V((1024, 128), bf), V((1152, 128), bf), V((1040, 128), f32), V((1024, 128), bf),
             V((128, 512), f32), V((4, 256, 256), bf), V((4, 256, 256), bf), V((2, 128, 256), bf),
-            V((4, 128, 512), bf), V((4, 128, 512), bf), V((256, 2048), f32), V((128, 2048), bf),
+            V((4, 128, 512), bf), V((4, 128, 512), bf), V((256, 2048), f32), V((128, 2048), bf), V((1024, 640), f32),
             dma((4,)), dma((4,)),
             dma((7,)), dma((5, 2, 8)), dma((3, 17, 3)), dma((2, 3)),
             dma((1,)), dma((4, 3)), dma((4, 4)), dma((3,)), dma((2, 2, 8)),

time: 77.1 us -> 71.6 us (0.929)
  Pallas kernels: 75.1 us -> 69.5 us
    pallas_call x1, Pallas kernels: 75.1 us -> 69.5 us  [on_device(): pl.pallas_call(kernel, out_shape=jax.ShapeDtypeStruct((128, 2048), bf), i...]
where the time goes in v3:
time: 71.6 us; the launch traced here: 71.4 us
  Pallas kernels  69.5 us (97%)
  local copies, waits for them, and re-layouts  1.88 us (3%)
    pallas_call x1, Pallas kernels, on_device(): pl.pallas_call(kernel, out_shape=jax.ShapeDtypeStruct((128, 2048), bf), i...  69.5 us
    unnamed x1, local copies, waits for them, and re-layouts  1.88 us

profile of v3, /device:TPU:1, one launch (start us, length us, event | category | flops | bytes accessed | tf_op | source)
XLA Modules:
  0.0 71.4 jit_solution(3796448626710934997)
XLA Ops:
  0.0 69.5 %shard_map.118 = bf16[128,2048]{1,0:T(8,128)(2,1)} custom-call(bf16[1024,256]{1,0:T(8,128)(2,1)} %bitcast.7, f32[1,2048]{1,0:T(1,128)} %bitcast.8, bf16[32,128]{1,0:T(8,128)(2,1)} %wq.1, bf16[32,64]{1,0:T(8,128)(2,1)} %wk.1, bf16[32,64]{1,0:T(8,128)(2,1)} %wv.1, bf16[32,128]{1,0:T(8,128)(2,1)} %wi.1, bf16[32,128]{1,0:T(8,128)(2,1)} %wb.1, ...), custom_call_target="tpu_custom_call" | custom-call | tf_op jit(solution)/shard_map/pallas_call | solution.py:528
  69.6 1.9 %copy.14 = bf16[1,128,2048]{2,1,0:T(8,128)(2,1)} copy(bf16[1,128,2048]{2,1,0:T(8,128)(2,1)} %bitcast.6) | data formatting | bytes 1048576

commit v4 on v3

--- a/solution.py
+++ b/solution.py
@@ -16,17 +16,17 @@
 
 STREAMS = (("zy", 256), ("zy", 384), ("zy", 256), ("yz", 256), ("yz", 512))
 UP = (8, 7, 8, 7, 8)
-SKIP = ((6, 2), (6, 2), (6, 2), (6, 2), (6, 2))
-DIRECT = 7
+SKIP = ((5, 3), (5, 3), (6, 2), (6, 2), (6, 2))
+DIRECT = 8
 LATE = 96
-EARLY = 4
+EARLY = (1, 2, 3, 4, 5)
 
 
 def kernel(
-    tok, gain, wq, wk, wv, wi, wb, wc, taps, sinks, wao, wco,
+    tok, gain_in, wq, wk, wv, wi, wb, wc, taps_in, sinks_in, wao, wco,
     out,
-    T, N, B0, B1, B2, B3, B4, Q, KV, PR, GB, BIAS, AALL, AOUT, RLY, XS, XR, ACC, OUTV, PACC,
-    lsem, osem, ss, zr, yr, ayr, tsem, xr, dr, oxr, xlr, hsem, hr, asem, ar, rr, es, er,
+    T, N, B0, B1, B2, B3, B4, Q, KV, PR, GB, BIAS, AALL, AOUT, RLY, XS, XR, ACC, OUTV, PACC, gain, taps, sinks, kvw,
+    lsem, wsem, osem, ss, zr, yfr, ynr, ayr, tsem, xr, dr, oxr, xlr, hsem, hr, asem, ar, rr, es, er,
 ):
     z = lax.axis_index("sp")
     y = lax.axis_index("fs")
@@ -54,23 +54,38 @@
     for peer in peers:
         pl.semaphore_signal(barrier, inc=1, device_id=peer, device_id_type=MESH)
 
+    own = pl.ds(pl.multiple_of(32 * (NY * z + y), 32), 32)
+    whole = (
+        (wq, B0, 0), (wi, B1, 0), (wb, B1, 128), (wc, B1, 256), (wao, B3, 0), (wco, B3, 128),
+    )
+    for src, buf, at in whole:
+        pltpu.make_async_copy(src, buf.at[own, at : at + 128], wsem.at[0]).start()
+    narrow = [pltpu.make_async_copy(src, kvw.at[k], wsem.at[1 + k]) for k, src in enumerate((wk, wv))]
+    small = [
+        pltpu.make_async_copy(src, dst, wsem.at[3 + k])
+        for k, (src, dst) in enumerate(((gain_in, gain), (taps_in, taps), (sinks_in, sinks)))
+    ]
+
     def tload(i):
         rows = pl.ds(256 * i, 256)
         return pltpu.make_async_copy(tok.at[rows, :], T.at[t, rows, :], lsem.at[i])
 
+    for copy in narrow:
+        copy.start()
     for i in range(4):
-        with jax.named_scope("load"):
-            tload(i).start()
-
-    own = pl.ds(pl.multiple_of(32 * (NY * z + y), 32), 32)
-    B0[own, 0:128] = wq[...]
-    B0[own, 128:256] = jnp.concatenate([wk[...], wv[...]], axis=1)
-    B1[own, 0:128] = wi[...]
-    B1[own, 128:256] = wb[...]
-    B1[own, 256:384] = wc[...]
-    B3[own, 0:128] = wao[...]
-    B3[own, 128:256] = wco[...]
-
+        tload(i).start()
+    for copy in small:
+        copy.start()
+    for copy in narrow:
+        copy.wait()
+    B0[own, 128:256] = jnp.concatenate([kvw[0], kvw[1]], axis=1)
+
+    def landed(ref, sem):
+        pltpu.make_async_copy(ref, ref, sem).wait()
+
+    landed(B1.at[0:64, :], wsem.at[0])
+    for copy in small:
+        copy.wait()
     with jax.named_scope("barrier"):
         pl.semaphore_wait(barrier, len(peers))
 
@@ -91,10 +106,6 @@
 
     def origin(way, s):
         return lax.rem(z + NZ - s, NZ) if way == 0 else lax.rem(z + s, NZ)
-
-    def zarrived(st, way, d):
-        ref = zblock(st, origin(way, d))
-        return rc(ref, ref, ss.at[st], zr.at[st, way, d - 1], dev(dz=1))
 
     def zpass(st, d):
         near, jump = SKIP[st]
@@ -107,94 +118,88 @@
                     continue
                 if d <= last:
                     rc(
-                        ref, ref, ss.at[st], zr.at[st, way, to - 1], dev(dz=hops if way == 0 else -hops)
+                        ref, ref, ss.at[st], zr.at[st, to - 1], dev(dz=hops if way == 0 else -hops)
                     ).start()
 
     def zs(st):
         zpass(st, 0)
 
     def zv(st, d):
-        for way in (0, 1):
-            if d <= steps(st, way):
-                zarrived(st, way, d).wait_recv()
+        rows = 32 if STREAMS[st][0] == "zy" else 128 - LATE if st == 4 else 128
+        ways = sum(d <= steps(st, way) for way in (0, 1))
+        landed(bufs[st].at[0 : ways * rows, :], zr.at[st, d - 1])
         zpass(st, d)
-        if st == 3:
-            xl_send(d - 1)
 
     def slots(st, s):
         if s < 0:
             return [(0, 0, 0)]
         return [(1 + 8 * way + s, way, s + 1) for way in (0, 1) if s < steps(st, way)]
 
-    def ycopy(st, slot, b, d, k, recv):
-        if k == 2 and d >= DIRECT:
-            ref = yblock(st, b, 2 if recv else 0)
-            to = dev(dy=2)
-        elif k == 2:
-            fwd_up = slot < 9
-            if recv:
-                ref = yblock(st, b, 2)
-            else:
-                ref = yblock(st, b, -1 if fwd_up else 1)
-            to = dev(dy=1 if fwd_up else -1)
+    def group(st, e):
+        return 0 if st == 2 or e in EARLY else 1
+
+    def y_start(st, slot, b, d, k):
+        up = slot < 9
+        if k == 2:
+            ref = yblock(st, b, 0 if d >= DIRECT else -1 if up else 1)
+            to = dev(dy=2 if d >= DIRECT else 1 if up else -1)
         else:
-            ref = yblock(st, b, 0 if not recv else (-1 if k == 0 else 1))
-            to = dev(dy=1 if k == 0 else -1)
-        return rc(ref, ref, ss.at[st], yr.at[st, slot, k], to)
+            ref = yblock(st, b, 0)
+            to = dev(dy=1 - 2 * k)
+        forwards = d < DIRECT and k == (0 if up else 1)
+        sem = yfr.at[st, d] if forwards else ynr.at[st, group(st, d)]
+        rc(ref, ref, ss.at[st], sem, to).start()
 
     def ys(st, e):
         for slot, way, d in slots(st, e - 1):
             for k in (0, 1, 2) if e >= DIRECT else (0, 1):
-                ycopy(st, slot, origin(way, d), d, k, False).start()
+                y_start(st, slot, origin(way, d), d, k)
 
     def yf(st, e):
-        for slot, way, d in slots(st, e - 1):
-            b = origin(way, d)
-            ycopy(st, slot, b, d, 0 if slot < 9 else 1, True).wait_recv()
-            ycopy(st, slot, b, d, 2, False).start()
-
-    def yn(st, e):
-        for slot, way, d in slots(st, e - 1):
-            b = origin(way, d)
-            ycopy(st, slot, b, d, 1 if slot < 9 else 0, True).wait_recv()
-            ycopy(st, slot, b, d, 2, True).wait_recv()
-            if e >= DIRECT:
-                ycopy(st, slot, b, d, 0 if slot < 9 else 1, True).wait_recv()
-
-    def aycopy(st, k, recv):
+        blocks = slots(st, e - 1)
+        landed(bufs[st].at[0 : 32 * len(blocks), :], yfr.at[st, e])
+        for slot, way, d in blocks:
+            y_start(st, slot, origin(way, d), d, 2)
+
+    def yw(st, g):
+        count = sum(
+            len(slots(st, e - 1)) * (3 if e >= DIRECT else 2) for e in range(9) if group(st, e) == g
+        )
+        landed(bufs[st].at[0 : 32 * count, :], ynr.at[st, g])
+
+    def ay_start(st, k):
         up = st % 2 == 0
         if k == 2:
-            ref = yblock(st, z, 2) if recv else yblock(st, z, -1 if up else 1)
+            ref = yblock(st, z, -1 if up else 1)
             to = dev(dy=1 if up else -1)
         else:
-            ref = yblock(st, z, 0 if not recv else (-1 if k == 0 else 1))
-            to = dev(dy=1 if k == 0 else -1)
-        return rc(ref, ref, ss.at[st], ayr.at[st - 3, k], to)
+            ref = yblock(st, z, 0)
+            to = dev(dy=1 - 2 * k)
+        rc(ref, ref, ss.at[st], ayr.at[st - 3, 0 if k == (0 if up else 1) else 1], to).start()
 
     def ay(st):
-        aycopy(st, 0, False).start()
-        aycopy(st, 1, False).start()
+        ay_start(st, 0)
+        ay_start(st, 1)
 
     def ayf(st):
-        aycopy(st, 0 if st % 2 == 0 else 1, True).wait_recv()
-        aycopy(st, 2, False).start()
+        landed(bufs[st].at[0:32, :], ayr.at[st - 3, 0])
+        ay_start(st, 2)
 
     def aye(st):
-        aycopy(st, 1 if st % 2 == 0 else 0, True).wait_recv()
-        aycopy(st, 2, True).wait_recv()
+        landed(bufs[st].at[0:64, :], ayr.at[st - 3, 1])
         zs(st)
 
     ox_parts = ((1, 4, 0), (2, 2, 0), (3, 4, 256))
 
     def oxcopy(k):
         d, st, at = ox_parts[k]
-        return rc(B3.at[own, :], bufs[st].at[own, at : at + 256], ss.at[5], oxr.at[k], dev(dx=-d))
+        return rc(B3.at[own, :], bufs[st].at[own, at : at + 256], ss.at[5], oxr.at[0], dev(dx=-d))
 
     def xlcopy(s, way, k):
         rows = pl.ds(pl.multiple_of(128 * origin(way, s + 1), 128), LATE)
         at = 256 * k
         return rc(
-            B3.at[rows, :], B4.at[rows, at : at + 256], ss.at[5 + k], xlr.at[k, way, s], dev(dx=-1 if k == 0 else 1)
+            B3.at[rows, :], B4.at[rows, at : at + 256], ss.at[5 + k], xlr.at[0], dev(dx=-1 if k == 0 else 1)
         )
 
     def xl_send(s):
@@ -202,12 +207,6 @@
             if s < steps(3, way):
                 for k in (0, 1):
                     xlcopy(s, way, k).start()
-
-    def xl_wait(s):
-        for way in (0, 1):
-            if s < steps(3, way):
-                for k in (0, 1):
-                    xlcopy(s, way, k).wait_recv()
 
     def tchunk(i, dx, cc):
         tt = lax.rem(x + NX + dx, NX) * 2 + cc
@@ -225,7 +224,7 @@
 
     def dcopy(i, k, recv):
         ref = tchunk(i, (0, -1, 1, 2)[k], c if not recv else 1 - c)
-        return rc(ref, ref, tsem.at[0], dr.at[i, k], partner)
+        return rc(ref, ref, tsem.at[0], dr.at[i], partner)
 
     def ts(i):
         tload(i).wait()
@@ -249,33 +248,24 @@
         dcopy(i, 3, False).start()
 
     def td(i):
-        for k in range(4):
-            dcopy(i, k, True).wait_recv()
+        landed(T.at[0], dr.at[i])
 
     def norm(i, h):
-        base = 256 * i + 64 * h
-
-        @pl.loop(0, 2)
-        def _(j):
-            rows = [pl.ds(pl.multiple_of(base + 32 * j + 16 * g, 16), 16) for g in range(2)]
-            averages, scales = [], []
-            for r in rows:
-                total = T[0, r, :].astype(jnp.float32)
-                for k in range(1, 8):
-                    total += T[k, r, :].astype(jnp.float32)
-                averages.append(jnp.sum(total, axis=1, keepdims=True) * (1.0 / 2048))
-            for r, average in zip(rows, averages):
-                squares = None
-                for k in range(8):
-                    centred = T[k, r, :].astype(jnp.float32) - average
-                    squares = centred * centred if k == 0 else squares + centred * centred
-                variance = jnp.sum(squares, axis=1, keepdims=True) * (1.0 / 2048)
-                scales.append(lax.rsqrt(variance + 1e-05))
-            for k in range(8):
-                cols = slice(256 * k, 256 * k + 256)
-                for r, average, scale in zip(rows, averages, scales):
-                    centred = T[k, r, :].astype(jnp.float32) - average
-                    N[r, cols] = (centred * scale * gain[:, cols]).astype(jnp.bfloat16)
+        rows = slice(256 * i + 128 * h, 256 * i + 128 * h + 128)
+        total = T[0, rows, :].astype(jnp.float32)
+        for k in range(1, 8):
+            total += T[k, rows, :].astype(jnp.float32)
+        average = jnp.sum(total, axis=1, keepdims=True) * (1.0 / 2048)
+        squares = None
+        for k in range(8):
+            centred = T[k, rows, :].astype(jnp.float32) - average
+            squares = centred * centred if k == 0 else squares + centred * centred
+        variance = jnp.sum(squares, axis=1, keepdims=True) * (1.0 / 2048)
+        scale = lax.rsqrt(variance + 1e-05)
+        for k in range(8):
+            cols = slice(256 * k, 256 * k + 256)
+            centred = T[k, rows, :].astype(jnp.float32) - average
+            N[rows, cols] = (centred * scale * gain[:, cols]).astype(jnp.bfloat16)
 
     def part(i, pairs):
         rows = slice(256 * i, 256 * i + 256)
@@ -295,13 +285,13 @@
 
     def pe(i):
         rows = slice(256 * i, 256 * i + 256)
-        qkv, ibc = part(i, [(d, d) for d in range(1, EARLY + 1)])
+        qkv, ibc = part(i, [(d, d) for d in EARLY])
         PACC[rows, 0:256] = qkv
         PACC[rows, 256:640] = ibc
 
     def proj(i):
         rows = slice(256 * i, 256 * i + 256)
-        qkv, ibc = part(i, [(d, d) for d in range(EARLY + 1, 8)] + [(0, 8)])
+        qkv, ibc = part(i, [(d, d) for d in range(1, 8) if d not in EARLY] + [(0, 8)])
         qkv = (qkv + PACC[rows, 0:256]).astype(jnp.bfloat16)
         ibc = (ibc + PACC[rows, 256:640]).astype(jnp.bfloat16)
         Q[rows, :] = qkv[:, 0:128]
@@ -376,11 +366,11 @@
         half = pl.ds(128 * u, 128)
         if k == 2:
             return rc(AOUT.at[k, half, :], RLY.at[u], asem.at[0], rr.at[u], dev(dx=1 - 2 * u))
-        return rc(AOUT.at[k, half, :], AALL.at[NX - k, half, :], asem.at[0], ar.at[k - 1, u], dev(dx=k))
+        return rc(AOUT.at[k, half, :], AALL.at[NX - k, half, :], asem.at[0], ar.at[k - 1], dev(dx=k))
 
     def relay(u):
         half = pl.ds(128 * u, 128)
-        return rc(RLY.at[u], AALL.at[2, half, :], asem.at[1], ar.at[1, u], dev(dx=1 - 2 * u))
+        return rc(RLY.at[u], AALL.at[2, half, :], asem.at[1], ar.at[1], dev(dx=1 - 2 * u))
 
     def out_dot(left, buf, n, at):
         right = buf[512 * n : 512 * n + 512, at : at + 256]
@@ -391,7 +381,7 @@
 
     def store(n):
         cols = slice(512 * n, 512 * n + 512)
-        return pltpu.make_async_copy(OUTV.at[:, cols], out.at[:, cols], osem.at[n])
+        return pltpu.make_async_copy(OUTV.at[:, cols], out.at[:, cols], osem.at[0])
 
     def start():
         bias_init()
@@ -401,11 +391,13 @@
             oxcopy(k).start()
 
     def oxw():
-        for k in range(3):
-            oxcopy(k).wait_recv()
-
-    def xw(d):
-        xl_wait(d - 1)
+        landed(B3.at[0:96, :], oxr.at[0])
+
+    def xs(d):
+        xl_send(d - 1)
+
+    def xw():
+        landed(B4.at[0 : 15 * LATE, :], xlr.at[0])
 
     def hs():
         halo(0).start()
@@ -425,8 +417,7 @@
         relay(u).start()
 
     def aw(k):
-        for u in (0, 1):
-            (relay(u) if k == 2 else acopy(k, u)).wait_recv()
+        landed(AALL.at[0], ar.at[k - 1])
 
     def f0():
         for n in range(4):
@@ -466,27 +457,24 @@
                 store(n - 1).start()
 
     order = (
-        (start,), (zs, 0), (ox,), (ts, 1), (ay, 3), (zs, 1), (ys, 0, 0), (ys, 1, 0), (zv, 0, 1), (oxw,), (ts, 0),
-        (zs, 2), (ay, 4), (ayf, 3), (zv, 1, 1), (ts, 3), (zv, 0, 2), (ayf, 4), (ts, 2), (zv, 2, 1), (ys, 1, 1),
-        (zv, 1, 2), (aye, 3), (zv, 0, 3), (tg, 0), (yf, 1, 0), (aye, 4), (tf, 0), (ys, 1, 2), (ys, 0, 3), (zv, 1, 3),
-        (ys, 0, 2), (zv, 2, 2), (tf, 3), (tg, 3), (ys, 1, 3), (zv, 0, 4), (zv, 3, 1), (ys, 0, 1), (yf, 1, 2),
-        (zv, 4, 1), (yf, 1, 1), (zv, 1, 4), (zv, 2, 3), (ys, 1, 4), (yf, 0, 3), (zv, 0, 5), (ys, 0, 5), (tf, 2),
-        (tf, 1), (th, 3), (ys, 0, 4), (zv, 3, 2), (th, 0), (ys, 2, 0), (yn, 1, 2), (yf, 0, 2), (yf, 0, 0), (ys, 2, 3),
-        (zv, 4, 2), (zv, 2, 4), (zv, 1, 5), (yf, 1, 3), (ys, 1, 5), (yf, 0, 4), (td, 3), (yf, 0, 1), (ys, 2, 4),
-        (tg, 2), (yf, 0, 5), (norm, 3, 2), (yf, 1, 4), (th, 2), (yn, 0, 3), (zv, 3, 3), (zv, 0, 6), (zv, 0, 7),
-        (ys, 0, 6), (norm, 3, 3), (norm, 3, 0), (yn, 0, 0), (th, 1), (tg, 1), (zv, 2, 5), (yn, 1, 1), (ys, 0, 7),
-        (td, 2), (norm, 2, 0), (norm, 2, 3), (zv, 1, 6), (zv, 4, 3), (td, 0), (ys, 1, 6), (td, 1), (norm, 1, 1),
-        (yf, 1, 5), (yn, 0, 5), (zv, 1, 7), (yn, 0, 1), (yn, 1, 3), (ys, 1, 7), (zv, 3, 4), (yn, 0, 2), (yn, 1, 4),
-        (norm, 1, 0), (norm, 0, 1), (yn, 0, 4), (norm, 0, 3), (xw, 1), (zv, 0, 8), (norm, 3, 1), (norm, 0, 0),
-        (yf, 0, 6), (zv, 2, 6), (ys, 0, 8), (xw, 3), (norm, 0, 2), (yf, 1, 6), (norm, 1, 3), (zv, 2, 7), (zv, 4, 4),
-        (yn, 1, 0), (zv, 1, 8), (yn, 0, 7), (ys, 1, 8), (zv, 3, 5), (norm, 1, 2), (pe, 1), (norm, 2, 1), (yn, 1, 5),
-        (pe, 3), (xw, 4), (yf, 2, 4), (ys, 2, 1), (norm, 2, 2), (ys, 2, 6), (pe, 0), (yn, 1, 6), (yn, 1, 7),
-        (yn, 0, 8), (yf, 2, 3), (yn, 0, 6), (yn, 1, 8), (proj, 3), (ys, 2, 5), (hs,), (zv, 3, 6), (pe, 2), (ys, 2, 2),
-        (ys, 2, 7), (proj, 0), (proj, 2), (proj, 1), (yn, 2, 3), (xw, 5), (zv, 4, 5), (zv, 3, 7), (zv, 2, 8), (hw,),
-        (mix, 2), (asend, 2), (yf, 2, 5), (mix, 3), (asend, 3), (mix, 1), (asend, 1), (yf, 2, 0), (yf, 2, 6),
-        (yf, 2, 1), (yn, 2, 4), (mix, 0), (ys, 2, 8), (zv, 3, 8), (zv, 4, 6), (xw, 7), (yn, 2, 5), (f0,), (yf, 2, 2),
-        (xw, 2), (af, 0), (xw, 6), (af, 1), (aw, 3), (yn, 2, 2), (yn, 2, 1), (yn, 2, 6), (aw, 1), (yn, 2, 7),
-        (zv, 4, 8), (zv, 4, 7), (yn, 2, 8), (yn, 2, 0), (xw, 8), (f1,), (f3,), (aw, 2), (ft,), (fo,), (comb,),
+        (start,), (ay, 3), (zs, 0), (zs, 1), (ys, 1, 0), (ys, 0, 0), (ox,), (ts, 2), (ayf, 3), (oxw,), (zs, 2),
+        (ts, 0), (ay, 4), (ts, 3), (zv, 0, 1), (zv, 1, 1), (yf, 0, 0), (ys, 0, 1), (aye, 3), (yf, 1, 0), (ayf, 4),
+        (zv, 2, 1), (tf, 2), (ys, 1, 1), (zv, 0, 2), (zv, 1, 2), (ys, 0, 2), (zv, 3, 1), (tg, 0), (ts, 1), (aye, 4),
+        (zv, 2, 2), (zv, 0, 3), (ys, 1, 2), (zv, 1, 3), (ys, 0, 3), (tf, 0), (ys, 2, 0), (yf, 0, 1), (zv, 3, 2),
+        (tf, 3), (zv, 4, 1), (yf, 1, 1), (tf, 1), (ys, 1, 3), (zv, 0, 4), (ys, 0, 4), (zv, 1, 4), (zv, 2, 3),
+        (ys, 1, 4), (tg, 2), (th, 2), (yf, 1, 2), (td, 2), (zv, 1, 6), (ys, 1, 6), (norm, 2, 0), (zv, 3, 3), (xs, 2),
+        (zv, 0, 6), (yf, 0, 4), (zv, 4, 2), (th, 0), (yf, 1, 3), (zv, 0, 5), (ys, 0, 5), (yf, 1, 4), (th, 3),
+        (yf, 0, 2), (zv, 1, 5), (zv, 0, 7), (th, 1), (tg, 1), (ys, 0, 7), (ys, 1, 5), (zv, 2, 4), (yf, 1, 6), (xs, 1),
+        (td, 1), (ys, 0, 6), (zv, 1, 7), (zv, 3, 4), (norm, 1, 1), (yf, 0, 3), (ys, 1, 7), (norm, 2, 1), (yf, 1, 5),
+        (xs, 3), (zv, 4, 3), (tg, 3), (yf, 0, 5), (td, 0), (zv, 1, 8), (zv, 0, 8), (ys, 0, 8), (yf, 0, 6), (td, 3),
+        (zv, 2, 5), (norm, 0, 1), (xs, 4), (ys, 1, 8), (zv, 3, 5), (yf, 0, 7), (yf, 2, 0), (norm, 0, 0), (yw, 1, 0),
+        (yw, 0, 0), (yf, 1, 7), (pe, 0), (ys, 2, 2), (norm, 1, 0), (pe, 2), (norm, 3, 0), (ys, 2, 4), (pe, 1),
+        (norm, 3, 1), (xs, 5), (zv, 4, 4), (ys, 2, 1), (yw, 0, 1), (pe, 3), (yw, 1, 1), (zv, 2, 7), (proj, 3),
+        (ys, 2, 3), (hs,), (zv, 2, 6), (yf, 2, 2), (zv, 3, 6), (proj, 2), (ys, 2, 5), (xs, 6), (proj, 1), (ys, 2, 6),
+        (ys, 2, 7), (proj, 0), (zv, 3, 7), (xs, 7), (yf, 2, 4), (zv, 4, 5), (yf, 2, 1), (hw,), (mix, 2), (asend, 2),
+        (zv, 2, 8), (mix, 1), (zv, 3, 8), (ys, 2, 8), (yf, 2, 5), (yf, 2, 7), (xs, 8), (asend, 1), (yf, 2, 3),
+        (mix, 3), (asend, 3), (zv, 4, 6), (mix, 0), (af, 0), (yf, 2, 6), (af, 1), (f0,), (aw, 3), (zv, 4, 7), (xw,),
+        (yw, 2, 0), (aw, 1), (zv, 4, 8), (f1,), (f3,), (aw, 2), (ft,), (fo,), (comb,),
     )
     for event, *where in order:
         with jax.named_scope(event.__name__ + "_".join(map(str, where))):
@@ -511,16 +499,13 @@
         sent(RLY, asem.at[1])
         sent(XS, es.at[0])
     with jax.named_scope("stored"):
-        for n in range(4):
-            store(n).wait()
+        pltpu.make_async_copy(OUTV, out, osem.at[0]).wait()
 
 
 def on_device(
     tokens, norm_gain, w_query, w_key, w_value, w_conv_in, w_conv_b, w_conv_c,
     conv_taps, sink_logits, w_attn_out, w_conv_out,
 ):
-    vmem = pl.BlockSpec(memory_space=pltpu.VMEM)
-    smem = pl.BlockSpec(memory_space=pltpu.SMEM)
     hbm = pl.BlockSpec(memory_space=pl.ANY)
     bf, f32 = jnp.bfloat16, jnp.float32
     dma = pltpu.SemaphoreType.DMA
@@ -528,7 +513,7 @@
     result = pl.pallas_call(
         kernel,
         out_shape=jax.ShapeDtypeStruct((128, 2048), bf),
-        in_specs=[hbm] + [vmem] * 8 + [smem] + [vmem] * 2,
+        in_specs=[hbm] * 12,
         out_specs=hbm,
         scratch_shapes=[
             V((8, 1024, 256), bf), V((1024, 2048), bf),
@@ -536,10 +521,11 @@
             V((1024, 128), bf), V((1152, 128), bf), V((1040, 128), f32), V((1024, 128), bf),
             V((128, 512), f32), V((4, 256, 256), bf), V((4, 256, 256), bf), V((2, 128, 256), bf),
             V((4, 128, 512), bf), V((4, 128, 512), bf), V((256, 2048), f32), V((128, 2048), bf), V((1024, 640), f32),
-            dma((4,)), dma((4,)),
-            dma((7,)), dma((5, 2, 8)), dma((3, 17, 3)), dma((2, 3)),
-            dma((1,)), dma((4, 3)), dma((4, 4)), dma((3,)), dma((2, 2, 8)),
-            dma((2,)), dma((2,)), dma((2,)), dma((3, 2)), dma((2,)), dma((1,)), dma((4,)),
+            V((1, 2048), f32), V((3, 128), bf), pltpu.SMEM((1, 2), f32), V((2, 32, 64), bf),
+            dma((4,)), dma((6,)), dma((1,)),
+            dma((7,)), dma((5, 8)), dma((3, max(DIRECT, 1))), dma((3, 2)), dma((2, 2)),
+            dma((1,)), dma((4, 3)), dma((4,)), dma((1,)), dma((1,)),
+            dma((2,)), dma((2,)), dma((2,)), dma((3,)), dma((2,)), dma((1,)), dma((4,)),
         ],
         compiler_params=pltpu.CompilerParams(
             collective_id=0, has_side_effects=True, vmem_limit_bytes=60 * 1024 * 1024

time: 71.6 us -> 69.1 us (0.965)
  Pallas kernels: 69.5 us -> 67.1 us
    pallas_call x1, Pallas kernels: 69.5 us -> 67.1 us  [on_device(): pl.pallas_call(kernel, out_shape=jax.ShapeDtypeStruct((128, 2048), bf), i...]
where the time goes in v4:
time: 69.1 us; the launch traced here: 69 us
  Pallas kernels  67.1 us (97%)
  local copies, waits for them, and re-layouts  1.88 us (3%)
    pallas_call x1, Pallas kernels, on_device(): pl.pallas_call(kernel, out_shape=jax.ShapeDtypeStruct((128, 2048), bf), i...  67.1 us
    unnamed x1, local copies, waits for them, and re-layouts  1.88 us

profile of v4, /device:TPU:1, one launch (start us, length us, event | category | flops | bytes accessed | tf_op | source)
XLA Modules:
  0.0 69.0 jit_solution(2874835653201407921)
XLA Ops:
  0.0 67.1 %shard_map.118 = bf16[128,2048]{1,0:T(8,128)(2,1)} custom-call(bf16[1024,256]{1,0:T(8,128)(2,1)} %bitcast.7, f32[1,2048]{1,0:T(1,128)} %bitcast.8, bf16[32,128]{1,0:T(8,128)(2,1)} %wq.1, bf16[32,64]{1,0:T(8,128)(2,1)} %wk.1, bf16[32,64]{1,0:T(8,128)(2,1)} %wv.1, bf16[32,128]{1,0:T(8,128)(2,1)} %wi.1, bf16[32,128]{1,0:T(8,128)(2,1)} %wb.1, ...), custom_call_target="tpu_custom_call" | custom-call | tf_op jit(solution)/shard_map/pallas_call | solution.py:513
  67.1 1.9 %copy.14 = bf16[1,128,2048]{2,1,0:T(8,128)(2,1)} copy(bf16[1,128,2048]{2,1,0:T(8,128)(2,1)} %bitcast.6) | data formatting | bytes 1048576

commit v5 on v4

--- a/solution.py
+++ b/solution.py
@@ -14,11 +14,11 @@
 MESH = pl.DeviceIdType.MESH
 NT = (((1,), (1,)), ((), ()))
 
-STREAMS = (("zy", 256), ("zy", 384), ("zy", 256), ("yz", 256), ("yz", 512))
-UP = (8, 7, 8, 7, 8)
-SKIP = ((5, 3), (5, 3), (6, 2), (6, 2), (6, 2))
-DIRECT = 8
-LATE = 96
+STREAMS = (("zy", 256), ("zy", 384), ("zy", 256), ("yz", 256), ("yz", 512), ("yz", 256))
+UP = (8, 7, 8, 7, 8, 7)
+SKIP = ((6, 2), (6, 2), (6, 2), (6, 2), (6, 2), (6, 2))
+DIRECT = 7
+LATE = 80
 EARLY = (1, 2, 3, 4, 5)
 
 
@@ -33,7 +33,7 @@
     t = lax.axis_index("tp")
     x = t // 2
     c = t % 2
-    bufs = (B0, B1, B2, B3, B4)
+    bufs = (B0, B1, B2, B3, B4, B3)
 
     def dev(dz=0, dy=0, dx=0):
         return (
@@ -95,7 +95,7 @@
             return buf.at[pl.ds(pl.multiple_of(32 * (NY * b + y), 32), 32), :]
         if st == 4:
             return buf.at[pl.ds(pl.multiple_of(128 * b + LATE, 16), 128 - LATE), :]
-        return buf.at[pl.ds(pl.multiple_of(128 * b, 128), 128), :]
+        return buf.at[pl.ds(pl.multiple_of(128 * b + (64 if st == 5 else 0), 64), 64), :]
 
     def yblock(st, b, dy):
         yy = lax.rem(y + NY + dy, NY)
@@ -118,14 +118,14 @@
                     continue
                 if d <= last:
                     rc(
-                        ref, ref, ss.at[st], zr.at[st, to - 1], dev(dz=hops if way == 0 else -hops)
+                        ref, ref, ss.at[3 if st == 5 else st], zr.at[st, to - 1], dev(dz=hops if way == 0 else -hops)
                     ).start()
 
     def zs(st):
         zpass(st, 0)
 
     def zv(st, d):
-        rows = 32 if STREAMS[st][0] == "zy" else 128 - LATE if st == 4 else 128
+        rows = 32 if STREAMS[st][0] == "zy" else 128 - LATE if st == 4 else 64
         ways = sum(d <= steps(st, way) for way in (0, 1))
         landed(bufs[st].at[0 : ways * rows, :], zr.at[st, d - 1])
         zpass(st, d)
@@ -457,24 +457,25 @@
                 store(n - 1).start()
 
     order = (
-        (start,), (ay, 3), (zs, 0), (zs, 1), (ys, 1, 0), (ys, 0, 0), (ox,), (ts, 2), (ayf, 3), (oxw,), (zs, 2),
-        (ts, 0), (ay, 4), (ts, 3), (zv, 0, 1), (zv, 1, 1), (yf, 0, 0), (ys, 0, 1), (aye, 3), (yf, 1, 0), (ayf, 4),
-        (zv, 2, 1), (tf, 2), (ys, 1, 1), (zv, 0, 2), (zv, 1, 2), (ys, 0, 2), (zv, 3, 1), (tg, 0), (ts, 1), (aye, 4),
-        (zv, 2, 2), (zv, 0, 3), (ys, 1, 2), (zv, 1, 3), (ys, 0, 3), (tf, 0), (ys, 2, 0), (yf, 0, 1), (zv, 3, 2),
-        (tf, 3), (zv, 4, 1), (yf, 1, 1), (tf, 1), (ys, 1, 3), (zv, 0, 4), (ys, 0, 4), (zv, 1, 4), (zv, 2, 3),
-        (ys, 1, 4), (tg, 2), (th, 2), (yf, 1, 2), (td, 2), (zv, 1, 6), (ys, 1, 6), (norm, 2, 0), (zv, 3, 3), (xs, 2),
-        (zv, 0, 6), (yf, 0, 4), (zv, 4, 2), (th, 0), (yf, 1, 3), (zv, 0, 5), (ys, 0, 5), (yf, 1, 4), (th, 3),
-        (yf, 0, 2), (zv, 1, 5), (zv, 0, 7), (th, 1), (tg, 1), (ys, 0, 7), (ys, 1, 5), (zv, 2, 4), (yf, 1, 6), (xs, 1),
-        (td, 1), (ys, 0, 6), (zv, 1, 7), (zv, 3, 4), (norm, 1, 1), (yf, 0, 3), (ys, 1, 7), (norm, 2, 1), (yf, 1, 5),
-        (xs, 3), (zv, 4, 3), (tg, 3), (yf, 0, 5), (td, 0), (zv, 1, 8), (zv, 0, 8), (ys, 0, 8), (yf, 0, 6), (td, 3),
-        (zv, 2, 5), (norm, 0, 1), (xs, 4), (ys, 1, 8), (zv, 3, 5), (yf, 0, 7), (yf, 2, 0), (norm, 0, 0), (yw, 1, 0),
-        (yw, 0, 0), (yf, 1, 7), (pe, 0), (ys, 2, 2), (norm, 1, 0), (pe, 2), (norm, 3, 0), (ys, 2, 4), (pe, 1),
-        (norm, 3, 1), (xs, 5), (zv, 4, 4), (ys, 2, 1), (yw, 0, 1), (pe, 3), (yw, 1, 1), (zv, 2, 7), (proj, 3),
-        (ys, 2, 3), (hs,), (zv, 2, 6), (yf, 2, 2), (zv, 3, 6), (proj, 2), (ys, 2, 5), (xs, 6), (proj, 1), (ys, 2, 6),
-        (ys, 2, 7), (proj, 0), (zv, 3, 7), (xs, 7), (yf, 2, 4), (zv, 4, 5), (yf, 2, 1), (hw,), (mix, 2), (asend, 2),
-        (zv, 2, 8), (mix, 1), (zv, 3, 8), (ys, 2, 8), (yf, 2, 5), (yf, 2, 7), (xs, 8), (asend, 1), (yf, 2, 3),
-        (mix, 3), (asend, 3), (zv, 4, 6), (mix, 0), (af, 0), (yf, 2, 6), (af, 1), (f0,), (aw, 3), (zv, 4, 7), (xw,),
-        (yw, 2, 0), (aw, 1), (zv, 4, 8), (f1,), (f3,), (aw, 2), (ft,), (fo,), (comb,),
+        (start,), (zs, 0), (ay, 3), (ox,), (zs, 1), (ts, 3), (ts, 2), (ys, 1, 0), (ayf, 3), (zv, 0, 1), (oxw,),
+        (ay, 4), (zs, 2), (zv, 1, 1), (ts, 1), (aye, 3), (zs, 5), (zv, 0, 2), (tf, 3), (ys, 0, 0), (ayf, 4), (ts, 0),
+        (zv, 2, 1), (ys, 1, 1), (ys, 0, 2), (zv, 1, 2), (zv, 3, 1), (ys, 1, 2), (zv, 5, 1), (yf, 1, 0), (zv, 0, 3),
+        (zv, 2, 2), (ys, 2, 2), (ys, 0, 1), (tg, 1), (zv, 1, 3), (aye, 4), (tg, 3), (ys, 0, 3), (zv, 3, 2),
+        (yf, 1, 2), (ys, 1, 3), (zv, 0, 4), (ys, 0, 4), (zv, 5, 2), (tg, 2), (yf, 0, 1), (zv, 1, 4), (zv, 2, 3),
+        (yf, 0, 2), (ys, 1, 4), (zv, 4, 1), (tf, 0), (yf, 1, 1), (yf, 0, 0), (zv, 3, 3), (yf, 1, 3), (th, 3), (tf, 2),
+        (zv, 0, 5), (tf, 1), (ys, 0, 5), (zv, 1, 5), (ys, 1, 5), (tg, 0), (zv, 5, 3), (yf, 1, 4), (yf, 0, 3),
+        (yf, 0, 4), (zv, 2, 4), (yf, 0, 5), (zv, 4, 2), (zv, 0, 6), (ys, 0, 6), (zv, 3, 4), (yf, 1, 5), (zv, 1, 6),
+        (ys, 1, 6), (zv, 0, 7), (ys, 0, 7), (th, 1), (td, 3), (zv, 5, 4), (th, 0), (yf, 0, 6), (th, 2), (xs, 4),
+        (zv, 1, 7), (ys, 1, 7), (zv, 2, 5), (norm, 3, 1), (td, 1), (zv, 4, 3), (yw, 0, 0), (zv, 0, 8), (ys, 0, 8),
+        (xs, 1), (td, 0), (zv, 3, 5), (norm, 3, 0), (zv, 1, 8), (ys, 1, 8), (yw, 1, 0), (zv, 5, 5), (yf, 1, 6),
+        (xs, 3), (pe, 3), (norm, 0, 0), (ys, 2, 3), (xs, 2), (td, 2), (norm, 1, 0), (zv, 2, 7), (zv, 4, 4),
+        (ys, 2, 7), (norm, 2, 1), (yw, 0, 1), (yf, 2, 2), (norm, 1, 1), (norm, 2, 0), (zv, 3, 6), (xs, 5), (yw, 1, 1),
+        (proj, 3), (hs,), (ys, 2, 0), (yf, 2, 3), (norm, 0, 1), (pe, 1), (zv, 5, 6), (ys, 2, 1), (zv, 2, 6), (xs, 6),
+        (pe, 2), (zv, 3, 7), (pe, 0), (zv, 5, 7), (zv, 4, 5), (xs, 7), (proj, 2), (proj, 0), (ys, 2, 6), (proj, 1),
+        (ys, 2, 5), (hw,), (mix, 2), (asend, 2), (yf, 2, 1), (ys, 2, 4), (mix, 1), (zv, 5, 8), (zv, 2, 8), (zv, 3, 8),
+        (xs, 8), (mix, 3), (yf, 2, 0), (asend, 1), (zv, 4, 6), (asend, 3), (ys, 2, 8), (yf, 2, 6), (mix, 0),
+        (yf, 2, 5), (yf, 2, 4), (f0,), (af, 0), (af, 1), (yw, 2, 0), (xw,), (zv, 4, 8), (aw, 3), (zv, 4, 7), (aw, 1),
+        (f1,), (f3,), (aw, 2), (ft,), (fo,), (comb,),
     )
     for event, *where in order:
         with jax.named_scope(event.__name__ + "_".join(map(str, where))):
@@ -523,7 +524,7 @@
             V((4, 128, 512), bf), V((4, 128, 512), bf), V((256, 2048), f32), V((128, 2048), bf), V((1024, 640), f32),
             V((1, 2048), f32), V((3, 128), bf), pltpu.SMEM((1, 2), f32), V((2, 32, 64), bf),
             dma((4,)), dma((6,)), dma((1,)),
-            dma((7,)), dma((5, 8)), dma((3, max(DIRECT, 1))), dma((3, 2)), dma((2, 2)),
+            dma((7,)), dma((6, 8)), dma((3, max(DIRECT, 1))), dma((3, 2)), dma((2, 2)),
             dma((1,)), dma((4, 3)), dma((4,)), dma((1,)), dma((1,)),
             dma((2,)), dma((2,)), dma((2,)), dma((3,)), dma((2,)), dma((1,)), dma((4,)),
         ],

time: 69.1 us -> 66.8 us (0.967)
  Pallas kernels: 67.1 us -> 64.8 us
    pallas_call x1, Pallas kernels: 67.1 us -> 64.8 us  [on_device(): pl.pallas_call(kernel, out_shape=jax.ShapeDtypeStruct((128, 2048), bf), i...]
where the time goes in v5:
time: 66.8 us; the launch traced here: 66.6 us
  Pallas kernels  64.8 us (97%)
  local copies, waits for them, and re-layouts  1.88 us (3%)
    pallas_call x1, Pallas kernels, on_device(): pl.pallas_call(kernel, out_shape=jax.ShapeDtypeStruct((128, 2048), bf), i...  64.8 us
    unnamed x1, local copies, waits for them, and re-layouts  1.88 us

profile of v5, /device:TPU:1, one launch (start us, length us, event | category | flops | bytes accessed | tf_op | source)
XLA Modules:
  0.0 66.6 jit_solution(5210812492456365751)
XLA Ops:
  0.0 64.8 %shard_map.118 = bf16[128,2048]{1,0:T(8,128)(2,1)} custom-call(bf16[1024,256]{1,0:T(8,128)(2,1)} %bitcast.7, f32[1,2048]{1,0:T(1,128)} %bitcast.8, bf16[32,128]{1,0:T(8,128)(2,1)} %wq.1, bf16[32,64]{1,0:T(8,128)(2,1)} %wk.1, bf16[32,64]{1,0:T(8,128)(2,1)} %wv.1, bf16[32,128]{1,0:T(8,128)(2,1)} %wi.1, bf16[32,128]{1,0:T(8,128)(2,1)} %wb.1, ...), custom_call_target="tpu_custom_call" | custom-call | tf_op jit(solution)/shard_map/pallas_call | solution.py:514
  64.8 1.9 %copy.14 = bf16[1,128,2048]{2,1,0:T(8,128)(2,1)} copy(bf16[1,128,2048]{2,1,0:T(8,128)(2,1)} %bitcast.6) | data formatting | bytes 1048576
